TPU v7x, 32 devices: a whole 2x2x4 slice. The times are simulated.
32 devices in a mesh: grp: 2 (over y), sp: 4 (over z), tp: 4 (over x, core).
Axes of the slice: x: 2, y: 2, z: 4, core: 2. Of those that a mesh axis runs over, the one named last changes fastest.
Arguments:
- target: bfloat16 [1024, 2048], P(('grp', 'sp', 'tp')), parts along dimension 0, may hold values from -60 to 60
- source: bfloat16 [8192, 2048], P(('grp', 'sp', 'tp')), parts along dimension 0, may hold values from -120 to 120
- w_query: bfloat16 [2, 2048, 2048], P(None, None, 'tp'), may hold values from -0.176776695 to 0.176776695
- w_key: bfloat16 [2, 2048, 2048], P(None, None, 'tp'), may hold values from -0.176776695 to 0.176776695
- w_value: bfloat16 [2, 2048, 2048], P(None, None, 'tp'), may hold values from -0.125 to 0.125
- w_out: bfloat16 [2, 2048, 2048], P(None, 'tp'), may hold values from -0.125 to 0.125
- gains: float32 [2, 2, 2048], replicated, may hold values from 0.1 to 1.9
Outputs:
- mixed: bfloat16 [1024, 2048], P(('grp', 'sp', 'tp')), parts along dimension 0
There are 2 independent parts, one for each index of `grp`. A program takes and returns all parts, laid end to end along the dimension named above; an argument that names none is the same for every part. Nothing has to cross between parts.
All inputs are finite; a program needn't handle non-finite values.
Results may differ from a plain program's by a relative error of at most 0.025.
Values may be sent and summed in bfloat16 or wider, within the bound.
A program may use at most 128 MiB of HBM per device.

v0:
```python
import functools
import math

import jax
import jax.numpy as jnp
from jax import lax
from jax.experimental import pallas as pl
from jax.experimental.pallas import tpu as pltpu
from jax.sharding import PartitionSpec as P

HEAD = 128
CORES = 2


EPS = 1e-06
MESH = pl.DeviceIdType.MESH
F32 = jnp.float32
BF16 = jnp.bfloat16


def normalize(row_block, gain_row):
    return (
        row_block
        * lax.rsqrt(jnp.mean(row_block * row_block, axis=-1, keepdims=True) + EPS)
        * gain_row
    )


def fused_kernel(
    nx, sp, depth,
    target, source, w_query, w_key, w_value, w_out, gains, out,
    tbuf, sbuf, wq, wk, wv, wo, keys, values, stream, normed, qbuf,
    osend, orecv, ssend, srecv, attended, pbuf, half_in, chip_sum, fin,
    local_sem, weight_sem, t_send, t_recv, t_fsend, s_psend, s_send, s_recv, s_fsend,
    q_send, q_recv, o_send, o_recv, e_send, e_recv,
    h_send, h_recv, c_send, c_psend, c_fsend, c_recv, c_frecv, f_send, f_recv,
):
    s = lax.axis_index("sp")
    t = lax.axis_index("tp")
    x = t // CORES
    c = t % CORES
    partner_c = 1 - c
    partner = {"tp": x * CORES + partner_c}
    units = sbuf.shape[0]
    half = sbuf.shape[2]
    width = sbuf.shape[3]
    rows = 2 * half
    local_width = wk.shape[2]
    heads = local_width // HEAD
    tp = nx * CORES
    trows = tbuf.shape[1]
    score_scale = HEAD ** (-0.5) * math.log2(math.e)

    def chip(step):
        return lax.rem(x + step, nx)

    def peer(step):
        return {"tp": chip(step) * CORES + c}

    def remote(src, dst, send_sem, recv_sem, device):
        return pltpu.make_async_remote_copy(
            src_ref=src, dst_ref=dst, send_sem=send_sem, recv_sem=recv_sem,
            device_id=device, device_id_type=MESH,
        )

    def arrived(dst, recv_sem):
        remote(dst, dst, t_send.at[0], recv_sem, partner).wait_recv()

    own_target = pltpu.make_async_copy(target, tbuf.at[t], local_sem.at[0])
    own_source = [
        pltpu.make_async_copy(
            source.at[pl.ds(part * half, half)], sbuf.at[0, part], local_sem.at[1 + part])
        for part in range(2)
    ]

    def load(kind, level):
        pair = ((w_query, wq), (w_key, wk), (w_value, wv), (w_out, wo))[kind]
        return pltpu.make_async_copy(
            pair[0].at[level], pair[1].at[level], weight_sem.at[kind, level])

    own_target.start()
    for copy in own_source:
        copy.start()
    load(1, 0).start()
    load(2, 0).start()

    barrier = pltpu.get_barrier_semaphore()
    pl.semaphore_signal(barrier, inc=1, device_id=partner, device_id_type=MESH)
    for step in range(1, nx):
        pl.semaphore_signal(barrier, inc=1, device_id=peer(step), device_id_type=MESH)
    for step in range(1, sp):
        pl.semaphore_signal(
            barrier, inc=1, device_id={"sp": lax.rem(s + step, sp)}, device_id_type=MESH)
    pl.semaphore_wait(barrier, 1 + (nx - 1) + (sp - 1))

    sends = []

    drains = []

    def finish():
        for drain in drains:
            drain()
        for copy in sends:
            copy.wait_send()

    def go(copy):
        copy.start()
        sends.append(copy)

    for step in range(1, nx):
        go(remote(target, tbuf.at[t], t_send.at[step], t_recv.at[t], peer(step)))
    go(remote(target, tbuf.at[t], t_send.at[0], t_recv.at[t], partner))
    for part in range(2):
        block = source.at[pl.ds(part * half, half)]
        for piece in range(2):
            span = pl.ds(piece * (half // 2), half // 2)
            for step in range(1, nx):
                unit = 2 * (nx - step) + part
                go(remote(block.at[span], sbuf.at[unit, 0, span], s_send.at[step, 2 * part + piece],
                          s_recv.at[unit, piece], peer(step)))
        go(remote(block, sbuf.at[1, part], s_psend.at[part], s_recv.at[1, part], partner))

    def project(index):
        unit = index // depth
        level = index % depth
        block = sbuf[unit].reshape(rows, width)
        start = pl.multiple_of(unit * rows, rows)
        k = jnp.dot(block, wk[level], preferred_element_type=F32)
        keys[level, pl.ds(start, rows), :] = k.astype(BF16)
        v = jnp.dot(block, wv[level], preferred_element_type=F32)
        values[level, :, pl.ds(start, rows)] = v.T.astype(BF16)

    def query_copy(level, step):
        return remote(qbuf.at[level, s], qbuf.at[level, s], q_send.at[level, step],
                      q_recv.at[level, s], {"sp": lax.rem(s + step, sp)})

    def drain_queries(level):
        for step in range(1, sp):
            query_copy(level, step).wait_send()

    def result_copies(level, j):
        return (
            remote(osend.at[level, j], orecv.at[level, s], o_send.at[level, j],
                   o_recv.at[level, s], {"sp": j}),
            remote(ssend.at[level, j], srecv.at[level, s], e_send.at[level, j],
                   e_recv.at[level, s], {"sp": j}),
        )

    def drain_results(level):
        for step in range(1, sp):
            for copy in result_copies(level, lax.rem(s + step, sp)):
                copy.wait_send()

    def target_relay(step):
        slot = chip(step) * CORES + c
        return remote(tbuf.at[slot], tbuf.at[slot], t_fsend.at[step], t_recv.at[slot], partner)

    def source_relay(unit, piece):
        span = pl.ds(piece * (half // 2), half // 2)
        return remote(sbuf.at[unit, 0, span], sbuf.at[unit, 1, span], s_fsend.at[unit, piece],
                      s_recv.at[unit, 2 + piece], partner)

    def drain_relays():
        for step in range(1, nx):
            target_relay(step).wait_send()
        for unit in range(2, units):
            for piece in range(2):
                source_relay(unit, piece).wait_send()

    def make_queries(level):
        q = jnp.dot(normed[...].reshape(tp * trows, width), wq[level], preferred_element_type=F32)
        qbuf[level, s] = q.astype(BF16)
        for step in range(1, sp):
            query_copy(level, step).start()

    def first_queries():
        own_target.wait()
        for step in range(1, nx):
            slot = chip(step) * CORES + c
            arrived(tbuf.at[slot], t_recv.at[slot])
            target_relay(step).start()
        for step in range(nx):
            slot = chip(step) * CORES + partner_c
            arrived(tbuf.at[slot], t_recv.at[slot])

        @pl.loop(0, tp)
        def _(block):
            value = tbuf[block].astype(F32)
            stream[block] = value
            normed[block] = normalize(value, gains[0, 0:1, :]).astype(BF16)

        load(0, 0).wait()
        make_queries(0)

    @pl.loop(0, units * depth - (depth - 1))
    def _(index):
        unit = index // depth
        level = index % depth

        @pl.when(index == 0)
        def _():
            for copy in own_source:
                copy.wait()
            load(1, 0).wait()
            load(2, 0).wait()
            load(0, 0).start()
            for later in range(1, depth):
                load(1, later).start()
                load(2, later).start()
            load(3, 0).start()
            for later in range(1, depth):
                load(0, later).start()
                load(3, later).start()

        for later in range(1, depth):
            @pl.when(index == later)
            def _():
                load(1, later).wait()
                load(2, later).wait()

        @pl.when(index == depth)
        def _():
            first_queries()
            for part in range(2):
                arrived(sbuf.at[1, part], s_recv.at[1, part])

        @pl.when(jnp.logical_and(unit >= 2, level == 0))
        def _():
            for piece in range(2):
                span = pl.ds(piece * (half // 2), half // 2)
                arrived(sbuf.at[unit, 0, span], s_recv.at[unit, piece])
                source_relay(unit, piece).start()
            for piece in range(2):
                span = pl.ds(piece * (half // 2), half // 2)
                arrived(sbuf.at[unit, 1, span], s_recv.at[unit, 2 + piece])

        project(index)

    drains += [drain_relays, functools.partial(drain_queries, 0)]

    both = jnp.minimum(s, sp - 1 - s)

    def near(i):
        side = jnp.where(i % 2 == 1, s - (i + 1) // 2, s + i // 2)
        rest = jnp.where(s < sp - 1 - s, i, sp - 1 - i)
        return jnp.where(i <= 2 * both, side, rest)

    for layer in range(depth):
        last = layer == depth - 1

        @pl.loop(0, sp)
        def _(i):
            j = near(sp - 1 - i if layer == 0 else i)

            @pl.when(j != s)
            def _():
                arrived(qbuf.at[layer, j], q_recv.at[layer, j])

            q = qbuf[layer, j]
            peaks, totals = [], []
            for h in range(heads):
                cols = slice(h * HEAD, (h + 1) * HEAD)
                scores = lax.dot_general(
                    keys[layer, :, cols], q[:, cols], (((1,), (1,)), ((), ())),
                    preferred_element_type=F32)
                peak = jnp.max(scores, axis=0, keepdims=True) * score_scale
                weights = jnp.exp2(scores * score_scale - peak)
                totals.append(jnp.sum(weights, axis=0, keepdims=True))
                peaks.append(peak)
                o = jnp.dot(values[layer, cols, :], weights.astype(BF16), preferred_element_type=F32)
                osend[layer, j, cols, :] = o.astype(BF16)
            ssend[layer, j] = jnp.concatenate(peaks + totals, axis=0)

            @pl.when(j != s)
            def _():
                for copy in result_copies(layer, j):
                    copy.start()

            @pl.when(j == s)
            def _():
                orecv[layer, s] = osend[layer, s]
                srecv[layer, s] = ssend[layer, s]

        drains.append(functools.partial(drain_results, layer))
        if layer == 0:
            @pl.loop(units * depth - (depth - 1), units * depth)
            def _(index):
                project(index)
        load(3, layer).wait()

        for step in range(1, sp):
            j = lax.rem(s + step, sp)
            arrived(orecv.at[layer, j], o_recv.at[layer, j])
            arrived(srecv.at[layer, j], e_recv.at[layer, j])
        peaks = [srecv[layer, j, 0:heads, :] for j in range(sp)]
        top = functools.reduce(jnp.maximum, peaks)
        share = [jnp.exp2(p - top) for p in peaks]
        total = sum(share[j] * srecv[layer, j, heads:2 * heads, :] for j in range(sp))
        share = [one / total for one in share]
        for h in range(heads):
            cols = slice(h * HEAD, (h + 1) * HEAD)
            mixed = sum(share[j][h:h + 1, :] * orecv[layer, j, cols, :].astype(F32) for j in range(sp))
            attended[:, cols] = mixed.T.astype(BF16)

        tile = min(512, width)
        for n in range(width // tile):
            cols = slice(n * tile, (n + 1) * tile)
            part = jnp.dot(attended[...], wo[layer, :, cols], preferred_element_type=F32)
            pbuf[layer, :, :, :, cols] = part.astype(BF16).reshape(nx, CORES, trows, tile)

        order = [chip(step) for step in list(range(1, nx)) + [0]]
        for b in order:
            go(remote(pbuf.at[layer, b, partner_c], half_in.at[layer, b], h_send.at[layer, b],
                      h_recv.at[layer, b], partner))
        if not last:
            for k, b in enumerate(order):
                arrived(half_in.at[layer, b], h_recv.at[layer, b])
                both_cores = pbuf[layer, b, c].astype(F32) + half_in[layer, b].astype(F32)
                chip_sum[layer, x, c, b] = both_cores.astype(BF16)
                own = chip_sum.at[layer, x, c, b]
                for step in range(1, nx):
                    go(remote(own, own, c_send.at[layer, step, k], c_recv.at[layer, x, b], peer(step)))
                go(remote(own, own, c_psend.at[layer, k], c_frecv.at[layer, x, b], partner))
            for step in range(1, nx):
                a = chip(step)
                for k in range(nx):
                    b = lax.rem(a + 1 + k, nx)
                    other = chip_sum.at[layer, a, c, b]
                    arrived(other, c_recv.at[layer, a, b])
                    go(remote(other, other, c_fsend.at[layer, step, k], c_frecv.at[layer, a, b], partner))
            for step in range(nx):
                a = chip(step)
                for k in range(nx):
                    b = lax.rem(a + 1 + k, nx)
                    arrived(chip_sum.at[layer, a, partner_c, b], c_frecv.at[layer, a, b])
            load(0, layer + 1).wait()

            @pl.loop(0, tp)
            def _(block):
                projected = sum(
                    chip_sum[layer, a, block % CORES, block // CORES].astype(F32) for a in range(nx))
                value = stream[block] + normalize(projected, gains[layer, 1:2, :])
                stream[block] = value
                normed[block] = normalize(value, gains[layer + 1, 0:1, :]).astype(BF16)

            make_queries(layer + 1)
            drains.append(functools.partial(drain_queries, layer + 1))
        else:
            for step in range(1, nx):
                b = chip(step)
                arrived(half_in.at[layer, b], h_recv.at[layer, b])
                both_cores = pbuf[layer, b, c].astype(F32) + half_in[layer, b].astype(F32)
                fin[0, b] = both_cores.astype(BF16)
                go(remote(fin.at[0, b], fin.at[1, x], f_send.at[step], f_recv.at[x], peer(step)))
            arrived(half_in.at[layer, x], h_recv.at[layer, x])
            projected = pbuf[layer, x, c].astype(F32) + half_in[layer, x].astype(F32)
            for step in range(1, nx):
                b = chip(step)
                arrived(fin.at[1, b], f_recv.at[b])
                projected = projected + fin[1, b].astype(F32)
            value = stream[t] + normalize(projected, gains[layer, 1:2, :])
            out[...] = value.astype(out.dtype)

    finish()


def fused_body(nx, sp, target, source, w_query, w_key, w_value, w_out, gains):
    depth, width, local_width = w_query.shape
    trows, rows = target.shape[0], source.shape[0]
    tp = nx * CORES
    block_rows = tp * trows
    heads = local_width // HEAD
    units = 2 * nx
    vmem = pltpu.VMEM
    dma = pltpu.SemaphoreType.DMA
    anywhere = pl.BlockSpec(memory_space=pl.ANY)
    whole = pl.BlockSpec(memory_space=pltpu.VMEM)
    return pl.pallas_call(
        functools.partial(fused_kernel, nx, sp, depth),
        out_shape=jax.ShapeDtypeStruct((trows, width), BF16),
        in_specs=[anywhere] * 6 + [whole],
        out_specs=whole,
        scratch_shapes=[
            vmem((tp, trows, width), BF16),
            vmem((units, 2, rows // 2, width), BF16),
            vmem(w_query.shape, BF16),
            vmem(w_key.shape, BF16),
            vmem(w_value.shape, BF16),
            vmem(w_out.shape, BF16),
            vmem((depth, units * rows, local_width), BF16),
            vmem((depth, local_width, units * rows), BF16),
            vmem((tp, trows, width), F32),
            vmem((tp, trows, width), BF16),
            vmem((depth, sp, block_rows, local_width), BF16),
            vmem((depth, sp, local_width, block_rows), BF16),
            vmem((depth, sp, local_width, block_rows), BF16),
            vmem((depth, sp, 2 * heads, block_rows), F32),
            vmem((depth, sp, 2 * heads, block_rows), F32),
            vmem((block_rows, local_width), BF16),
            vmem((depth, nx, CORES, trows, width), BF16),
            vmem((depth, nx, trows, width), BF16),
            vmem((depth, nx, CORES, nx, trows, width), BF16),
            vmem((2, nx, trows, width), BF16),
            dma((3,)), dma((4, depth)),
            dma((nx,)), dma((tp,)), dma((nx,)),
            dma((2,)), dma((nx, 4)), dma((units, 4)), dma((units, 2)),
            dma((depth, sp)), dma((depth, sp)),
            dma((depth, sp)), dma((depth, sp)), dma((depth, sp)), dma((depth, sp)),
            dma((depth, nx)), dma((depth, nx)),
            dma((depth, nx, nx)), dma((depth, nx)), dma((depth, nx, nx)),
            dma((depth, nx, nx)), dma((depth, nx, nx)),
            dma((nx,)), dma((nx,)),
        ],
        compiler_params=pltpu.CompilerParams(
            collective_id=0, has_side_effects=True, vmem_limit_bytes=60 * 1024 * 1024),
    )(target, source, w_query, w_key, w_value, w_out, gains)


def split_heads(row_block):
    return row_block.reshape(row_block.shape[0], row_block.shape[1] // HEAD, HEAD)


def body(target, source, w_query, w_key, w_value, w_out, gains):
    local_width = w_query.shape[2]
    score_scale = HEAD ** (-0.5)
    depth = w_query.shape[0]
    project_shard_part = lax.all_gather(source, "tp", axis=0, tiled=True)
    layer_parts = [
        jnp.stack(
            [
                jnp.dot(project_shard_part, w_key[level], preferred_element_type=jnp.float32),
                jnp.dot(project_shard_part, w_value[level], preferred_element_type=jnp.float32),
            ]
        )
        for level in range(depth)
    ]
    projected_source = jnp.stack(layer_parts).astype(jnp.bfloat16)
    stream = target.astype(jnp.float32)
    for layer_index in range(depth):
        normed = normalize(stream, gains[layer_index, 0]).astype(jnp.bfloat16)
        query_weight = w_query[layer_index]
        queries = jnp.dot(
            lax.all_gather(normed, "tp", axis=0, tiled=True),
            query_weight,
            preferred_element_type=jnp.float32,
        ).astype(jnp.bfloat16)
        row_count = queries.shape[0]
        keys_here = projected_source[layer_index, 0]
        values_here = projected_source[layer_index, 1]
        every_query = lax.all_gather(queries, "sp", axis=0, tiled=True)
        scores = (
            jnp.einsum(
                "qhd,khd->hqk",
                split_heads(every_query),
                split_heads(keys_here),
                preferred_element_type=jnp.float32,
            )
            * score_scale
        )
        row_peak = lax.pmax(jnp.max(scores, axis=2), "sp")
        weights = jnp.exp(scores - row_peak[:, :, None])
        local_summed = jnp.einsum(
            "hqk,khd->hqd",
            weights.astype(jnp.bfloat16),
            split_heads(values_here),
            preferred_element_type=jnp.float32,
        )
        summed, row_total = (
            lax.psum_scatter(
                local_summed.astype(jnp.bfloat16), "sp", scatter_dimension=1, tiled=True
            ).astype(jnp.float32),
            lax.psum_scatter(
                jnp.sum(weights, axis=2).astype(jnp.bfloat16), "sp", scatter_dimension=1, tiled=True
            ).astype(jnp.float32),
        )
        heads_out = summed / row_total[:, :, None]
        attended = (
            jnp.transpose(heads_out, (1, 0, 2)).reshape(row_count, local_width).astype(jnp.bfloat16)
        )
        out_weight = w_out[layer_index]
        projected = lax.psum_scatter(
            jnp.dot(attended, out_weight, preferred_element_type=jnp.float32).astype(jnp.bfloat16),
            "tp",
            scatter_dimension=0,
            tiled=True,
        ).astype(jnp.float32)
        stream = stream + normalize(projected, gains[layer_index, 1])
    return stream.astype(jnp.bfloat16)


def solution(mesh):
    in_specs = (
        P(("grp", "sp", "tp"), None),
        P(("grp", "sp", "tp"), None),
        P(None, None, "tp"),
        P(None, None, "tp"),
        P(None, None, "tp"),
        P(None, "tp", None),
        P(),
    )
    out_specs = P(("grp", "sp", "tp"), None)
    sp, tp = mesh.shape["sp"], mesh.shape["tp"]

    def run(target, source, w_query, w_key, w_value, w_out, gains):
        trows, rows, local_width = target.shape[0], source.shape[0], w_query.shape[2]
        tiles = (trows % 16 == 0 and (tp * trows) % 128 == 0 and rows % 128 == 0 and rows % 64 == 0
                 and local_width % (4 * HEAD) == 0 and tp % CORES == 0)
        form = functools.partial(fused_body, tp // CORES, sp) if tiles else body
        return form(target, source, w_query, w_key, w_value, w_out, gains)

    return jax.shard_map(run, mesh=mesh, in_specs=in_specs, out_specs=out_specs, check_vma=False)
```

profile of v0, /device:TPU:0, one launch (start us, length us, event | category | flops | bytes accessed | tf_op | source)
XLA Modules:
  0.0 96.3 jit_solution(3763415107744869442)
XLA Ops:
  0.0 94.8 %shard_map.73 = bf16[32,2048]{1,0:T(8,128)(2,1)} custom-call(bf16[32,2048]{1,0:T(8,128)(2,1)} %target.1, bf16[256,2048]{1,0:T(8,128)(2,1)} %source.1, bf16[2,2048,512]{2,1,0:T(8,128)(2,1)} %w_query.1, bf16[2,2048,512]{2,1,0:T(8,128)(2,1)} %w_key.1, bf16[2,2048,512]{2,1,0:T(8,128)(2,1)} %w_value.1, bf16[2,512,2048]{2,1,0:T(8,128)(2,1)} %w_out.1, ...), custom_call_target="tpu_custom_call" | custom-call | tf_op jit(solution)/shard_map/pallas_call | solution.py:378
  94.8 1.6 %copy.9 = bf16[32,2048]{1,0:T(8,128)(2,1)} copy(bf16[32,2048]{1,0:T(8,128)(2,1)} %shard_map.73) | data formatting | bytes 262144
where the time goes:
time: 96.5 us; the launch traced here: 96.3 us
  Pallas kernels  94.8 us (98%)
  local copies, waits for them, and re-layouts  1.57 us (2%)
    pallas_call x1, Pallas kernels, fused_body(): pl.pallas_call(functools.partial(fused_kernel, nx, sp, depth), out_shape=...  94.8 us

commit v1 on v0

v1 whole, which is shorter than its diff:
```python
import functools
import math

import jax
import jax.numpy as jnp
from jax import lax
from jax.experimental import pallas as pl
from jax.experimental.pallas import tpu as pltpu
from jax.sharding import PartitionSpec as P

HEAD = 128
CORES = 2
PIECES = 2


EPS = 1e-06
MESH = pl.DeviceIdType.MESH
F32 = jnp.float32
LOWEST = -1e30
BF16 = jnp.bfloat16


def normalize(row_block, gain_row):
    return (
        row_block
        * lax.rsqrt(jnp.mean(row_block * row_block, axis=-1, keepdims=True) + EPS)
        * gain_row
    )


def fused_kernel(
    nx, sp, depth,
    target, source, w_query, w_key, w_value, w_out, gains, out,
    tbuf, sbuf, wq, wk, wv, wo, keys, values, stream, normed, qbuf,
    osend, orecv, ssend, srecv, orelay, srelay, attended, pbuf, half_in, chip_sum, fin,
    local_sem, weight_sem, t_send, t_recv, t_fsend, s_psend, s_send, s_recv, s_fsend,
    q_send, q_recv, q_fsend, o_send, o_recv, e_send, e_recv, or_recv, er_recv,
    h_send, h_recv, c_send, c_psend, c_fsend, c_recv, c_frecv, f_send, f_recv,
):
    s = lax.axis_index("sp")
    t = lax.axis_index("tp")
    x = t // CORES
    c = t % CORES
    partner_c = 1 - c
    partner = {"tp": x * CORES + partner_c}
    units = sbuf.shape[0]
    half = sbuf.shape[2]
    width = sbuf.shape[3]
    rows = 2 * half
    local_width = wk.shape[2]
    heads = local_width // HEAD
    tp = nx * CORES
    prows = stream.shape[2]
    piece_rows = tp * prows
    score_scale = HEAD ** (-0.5) * math.log2(math.e)

    pairs = sp // 2
    edge = jnp.logical_or(s == 0, s == sp - 1)
    mirror = sp - 1 - s
    relays = jnp.logical_or(s == 1, s == sp - 2)
    relay_from = jnp.where(s == 1, 0, sp - 1)
    relay_to = sp - 1 - relay_from
    via = jnp.where(s == 0, 1, sp - 2)

    def chip(step):
        return lax.rem(x + step, nx)

    def peer(step):
        return {"tp": chip(step) * CORES + c}

    def remote(src, dst, send_sem, recv_sem, device):
        return pltpu.make_async_remote_copy(
            src_ref=src, dst_ref=dst, send_sem=send_sem, recv_sem=recv_sem,
            device_id=device, device_id_type=MESH,
        )

    def arrived(dst, recv_sem):
        remote(dst, dst, t_send.at[0], recv_sem, partner).wait_recv()

    own_target = pltpu.make_async_copy(target, tbuf.at[t], local_sem.at[0])
    own_source = [
        pltpu.make_async_copy(
            source.at[pl.ds(part * half, half)], sbuf.at[0, part], local_sem.at[1 + part])
        for part in range(2)
    ]

    def load(kind, level):
        pair = ((w_query, wq), (w_key, wk), (w_value, wv), (w_out, wo))[kind]
        return pltpu.make_async_copy(
            pair[0].at[level], pair[1].at[level], weight_sem.at[kind, level])

    own_target.start()
    for copy in own_source:
        copy.start()
    load(1, 0).start()
    load(2, 0).start()

    barrier = pltpu.get_barrier_semaphore()
    pl.semaphore_signal(barrier, inc=1, device_id=partner, device_id_type=MESH)
    for step in range(1, nx):
        pl.semaphore_signal(barrier, inc=1, device_id=peer(step), device_id_type=MESH)
    for step in range(1, sp):
        pl.semaphore_signal(
            barrier, inc=1, device_id={"sp": lax.rem(s + step, sp)}, device_id_type=MESH)
    with jax.named_scope("barrier"):
        pl.semaphore_wait(barrier, 1 + (nx - 1) + (sp - 1))

    sends = []

    drains = []

    def finish():
        for drain in drains:
            drain()
        for copy in sends:
            copy.wait_send()

    def go(copy):
        copy.start()
        sends.append(copy)

    for step in range(1, nx):
        go(remote(target, tbuf.at[t], t_send.at[step], t_recv.at[t], peer(step)))
    go(remote(target, tbuf.at[t], t_send.at[0], t_recv.at[t], partner))
    for part in range(2):
        block = source.at[pl.ds(part * half, half)]
        for piece in range(2):
            span = pl.ds(piece * (half // 2), half // 2)
            for step in range(1, nx):
                unit = 2 * (nx - step) + part
                go(remote(block.at[span], sbuf.at[unit, 0, span], s_send.at[step, 2 * part + piece],
                          s_recv.at[unit, piece], peer(step)))
        go(remote(block, sbuf.at[1, part], s_psend.at[part], s_recv.at[1, part], partner))

    def project(index):
        unit = index // depth
        level = index % depth
        with jax.named_scope("project"):
            block = sbuf[unit].reshape(rows, width)
            start = pl.multiple_of(unit * rows, rows)
            k = jnp.dot(block, wk[level], preferred_element_type=F32)
            keys[level, pl.ds(start, rows), :] = k.astype(BF16)
            v = jnp.dot(block, wv[level], preferred_element_type=F32)
            values[level, :, pl.ds(start, rows)] = v.T.astype(BF16)

    def far_pair(j):
        return jnp.logical_and(edge, j == mirror)

    def query_copy(level, p, step):
        return remote(qbuf.at[level, p, s], qbuf.at[level, p, s], q_send.at[level, p, step],
                      q_recv.at[level, p, s], {"sp": lax.rem(s + step, sp)})

    def query_relay(level, p):
        return remote(qbuf.at[level, p, relay_to], qbuf.at[level, p, relay_to],
                      q_fsend.at[level, p], q_recv.at[level, p, relay_to], {"sp": relay_from})

    def each_query(level, p, act):
        for step in range(1, sp):
            copy = query_copy(level, p, step)
            if level == 0:
                act(copy)
            else:
                @pl.when(jnp.logical_not(far_pair(lax.rem(s + step, sp))))
                def _():
                    act(copy)

    def send_queries(level, p):
        each_query(level, p, lambda copy: copy.start())

    def drain_queries(level):
        for p in range(PIECES):
            each_query(level, p, lambda copy: copy.wait_send())
            if level > 0:
                @pl.when(relays)
                def _():
                    query_relay(level, p).wait_send()

    def result_copies(level, p, j):
        return (
            remote(osend.at[level, p, j], orecv.at[level, p, s], o_send.at[level, p, j],
                   o_recv.at[level, p, s], {"sp": j}),
            remote(ssend.at[level, p, j], srecv.at[level, p, s], e_send.at[level, p, j],
                   e_recv.at[level, p, s], {"sp": j}),
        )

    def relay_copies(level, p, j):
        return (
            remote(osend.at[level, p, j], orelay.at[level, p], o_send.at[level, p, j],
                   or_recv.at[level, p], {"sp": via}),
            remote(ssend.at[level, p, j], srelay.at[level, p], e_send.at[level, p, j],
                   er_recv.at[level, p], {"sp": via}),
        )

    def drain_results(level):
        for p in range(PIECES):
            for step in range(1, sp):
                for copy in result_copies(level, p, lax.rem(s + step, sp)):
                    copy.wait_send()

    def target_relay(step):
        slot = chip(step) * CORES + c
        return remote(tbuf.at[slot], tbuf.at[slot], t_fsend.at[step], t_recv.at[slot], partner)

    def source_relay(unit, piece):
        span = pl.ds(piece * (half // 2), half // 2)
        return remote(sbuf.at[unit, 0, span], sbuf.at[unit, 1, span], s_fsend.at[unit, piece],
                      s_recv.at[unit, 2 + piece], partner)

    def drain_relays():
        for step in range(1, nx):
            target_relay(step).wait_send()
        for unit in range(2, units):
            for piece in range(2):
                source_relay(unit, piece).wait_send()

    def first_queries():
        own_target.wait()
        for step in range(1, nx):
            slot = chip(step) * CORES + c
            arrived(tbuf.at[slot], t_recv.at[slot])
            target_relay(step).start()
        for step in range(nx):
            slot = chip(step) * CORES + partner_c
            arrived(tbuf.at[slot], t_recv.at[slot])

        @pl.loop(0, tp)
        def _(block):
            value = tbuf[block].astype(F32)
            ready = normalize(value, gains[0, 0:1, :]).astype(BF16)
            for p in range(PIECES):
                span = slice(p * prows, (p + 1) * prows)
                stream[p, block] = value[span]
                normed[p, block] = ready[span]

        load(0, 0).wait()
        q = jnp.dot(normed[...].reshape(PIECES * piece_rows, width), wq[0],
                    preferred_element_type=F32)
        for p in range(PIECES):
            qbuf[0, p, s] = q[p * piece_rows:(p + 1) * piece_rows].astype(BF16)
            send_queries(0, p)

        @pl.when(edge)
        def _():
            lowest = jnp.full((heads, 2 * piece_rows), LOWEST, F32)
            empty = jnp.concatenate([lowest, jnp.zeros_like(lowest)], axis=0)
            for level in range(depth):
                for p in range(PIECES):
                    orecv[level, p, mirror] = jnp.zeros((piece_rows, local_width), BF16)
                    srecv[level, p, mirror] = empty

    @pl.loop(0, units * depth - (depth - 1))
    def _(index):
        unit = index // depth
        level = index % depth

        @pl.when(index == 0)
        def _():
            for copy in own_source:
                copy.wait()
            load(1, 0).wait()
            load(2, 0).wait()
            load(0, 0).start()
            for later in range(1, depth):
                load(1, later).start()
                load(2, later).start()
            load(3, 0).start()
            for later in range(1, depth):
                load(0, later).start()
                load(3, later).start()

        for later in range(1, depth):
            @pl.when(index == later)
            def _():
                load(1, later).wait()
                load(2, later).wait()

        @pl.when(index == depth)
        def _():
            with jax.named_scope("first_queries"):
                first_queries()
            for part in range(2):
                arrived(sbuf.at[1, part], s_recv.at[1, part])

        @pl.when(jnp.logical_and(unit >= 2, level == 0))
        def _():
            with jax.named_scope("wait_remote"):
                for piece in range(2):
                    span = pl.ds(piece * (half // 2), half // 2)
                    arrived(sbuf.at[unit, 0, span], s_recv.at[unit, piece])
                    source_relay(unit, piece).start()
                for piece in range(2):
                    span = pl.ds(piece * (half // 2), half // 2)
                    arrived(sbuf.at[unit, 1, span], s_recv.at[unit, 2 + piece])

        project(index)

    drains += [drain_relays, functools.partial(drain_queries, 0)]

    def columns(parts):
        stacked = jnp.concatenate(parts, axis=0)
        fill = jnp.zeros((HEAD - stacked.shape[0], stacked.shape[1]), F32)
        return jnp.concatenate([stacked, fill], axis=0).T

    def weighted(cols, blocks, h):
        span = slice(h * HEAD, (h + 1) * HEAD)
        return sum(
            cols[0:piece_rows, k * heads + h:k * heads + h + 1] * block[:, span].astype(F32)
            for k, block in enumerate(blocks))

    def merge(layer, p):
        @pl.when(relays)
        def _():
          with jax.named_scope("merge"):
            arrived(orelay.at[layer, p], or_recv.at[layer, p])
            arrived(srelay.at[layer, p], er_recv.at[layer, p])
            mine, theirs = ssend[layer, p, relay_to], srelay[layer, p]
            top = jnp.maximum(mine[0:heads], theirs[0:heads])
            share = [jnp.exp2(one[0:heads] - top) for one in (mine, theirs)]
            total = share[0] * mine[heads:] + share[1] * theirs[heads:]
            cols = columns(share)
            blocks = (osend[layer, p, relay_to], orelay[layer, p])
            for h in range(heads):
                osend[layer, p, relay_to, :, h * HEAD:(h + 1) * HEAD] = weighted(
                    cols, blocks, h).astype(BF16)
            ssend[layer, p, relay_to] = jnp.concatenate([top, total], axis=0)
            for copy in result_copies(layer, p, relay_to):
                copy.start()

    def attend(layer, p, pair):
        first = 2 * pair
        for member in range(2):
            j = first + member

            @pl.when(j != s)
            def _():
                with jax.named_scope("wait_q"):
                    arrived(qbuf.at[layer, p, j], q_recv.at[layer, p, j])

            if layer > 0:
                @pl.when(jnp.logical_and(relays, j == relay_to))
                def _():
                    query_relay(layer, p).start()

        with jax.named_scope("attend"):
            q = qbuf[layer, p, pl.ds(first, 2)].reshape(2 * piece_rows, local_width)
            peaks, totals = [], []
            for h in range(heads):
                cols = slice(h * HEAD, (h + 1) * HEAD)
                scores = lax.dot_general(
                    keys[layer, :, cols], q[:, cols], (((1,), (1,)), ((), ())),
                    preferred_element_type=F32)
                peak = jnp.max(scores, axis=0, keepdims=True) * score_scale
                weights = jnp.exp2(scores * score_scale - peak)
                totals.append(jnp.sum(weights, axis=0, keepdims=True))
                peaks.append(peak)
                o = jnp.dot(values[layer, cols, :], weights.astype(BF16), preferred_element_type=F32)
                o = o.T.astype(BF16)
                for member in range(2):
                    osend[layer, p, first + member, :, cols] = o[member * piece_rows:(member + 1) * piece_rows]
            stats = jnp.concatenate(peaks + totals, axis=0)
            ssend[layer, p, first] = stats
            ssend[layer, p, first + 1] = pltpu.roll(stats, piece_rows, 1)

        for member in (1, 0):
            j = first + member

            @pl.when(j == s)
            def _():
                orecv[layer, p, s] = osend[layer, p, s]
                srecv[layer, p, s] = ssend[layer, p, s]

            @pl.when(far_pair(j))
            def _():
                for copy in relay_copies(layer, p, j):
                    copy.start()

            held = jnp.logical_or(far_pair(j), jnp.logical_and(relays, j == relay_to))

            @pl.when(jnp.logical_not(jnp.logical_or(held, j == s)))
            def _():
                for copy in result_copies(layer, p, j):
                    copy.start()

    def out_project(layer, p):
        with jax.named_scope("wait_o"):
            for step in range(1, sp):
                j = lax.rem(s + step, sp)

                @pl.when(jnp.logical_not(far_pair(j)))
                def _():
                    arrived(orecv.at[layer, p, j], o_recv.at[layer, p, j])
                    arrived(srecv.at[layer, p, j], e_recv.at[layer, p, j])
        with jax.named_scope("combine_out"):
            stats = [srecv[layer, p, j] for j in range(sp)]
            top = functools.reduce(jnp.maximum, [one[0:heads] for one in stats])
            share = [jnp.exp2(one[0:heads] - top) for one in stats]
            total = sum(part * one[heads:] for part, one in zip(share, stats))
            cols = columns([part / total for part in share])
            blocks = [orecv[layer, p, j] for j in range(sp)]
            for h in range(heads):
                attended[:, h * HEAD:(h + 1) * HEAD] = weighted(cols, blocks, h).astype(BF16)
            tile = min(512, width)
            for n in range(width // tile):
                span = slice(n * tile, (n + 1) * tile)
                part = jnp.dot(attended[...], wo[layer, :, span], preferred_element_type=F32).astype(BF16)
                for b in range(nx):
                    for core in range(CORES):
                        at = (b * CORES + core) * prows
                        pbuf[layer, p, core, b, :, span] = part[at:at + prows]
            go(remote(pbuf.at[layer, p, partner_c], half_in.at[layer, p], h_send.at[layer, p],
                      h_recv.at[layer, p], partner))

    def chip_total(layer, p):
        with jax.named_scope("chip_total"):
            arrived(half_in.at[layer, p], h_recv.at[layer, p])
            for b in range(nx):
                both_cores = pbuf[layer, p, c, b].astype(F32) + half_in[layer, p, b].astype(F32)
                chip_sum[layer, p, x, c, b] = both_cores.astype(BF16)
            own = chip_sum.at[layer, p, x, c]
            for step in range(1, nx):
                go(remote(own, own, c_send.at[layer, p, step], c_recv.at[layer, p, x], peer(step)))
            go(remote(own, own, c_psend.at[layer, p], c_frecv.at[layer, p, x], partner))

    def next_queries(layer, p):
        with jax.named_scope("xwait"):
            for step in range(1, nx):
                a = chip(step)
                other = chip_sum.at[layer, p, a, c]
                arrived(other, c_recv.at[layer, p, a])
                go(remote(other, other, c_fsend.at[layer, p, step], c_frecv.at[layer, p, a], partner))
            for step in range(nx):
                a = chip(step)
                arrived(chip_sum.at[layer, p, a, partner_c], c_frecv.at[layer, p, a])
        with jax.named_scope("norm_q"):
            for block in range(tp):
                projected = sum(
                    chip_sum[layer, p, a, block % CORES, block // CORES].astype(F32) for a in range(nx))
                value = stream[p, block] + normalize(projected, gains[layer, 1:2, :])
                stream[p, block] = value
                normed[p, block] = normalize(value, gains[layer + 1, 0:1, :]).astype(BF16)
            q = jnp.dot(normed[p].reshape(piece_rows, width), wq[layer + 1],
                        preferred_element_type=F32)
            qbuf[layer + 1, p, s] = q.astype(BF16)
            send_queries(layer + 1, p)

    def final_send(layer, p):
        with jax.named_scope("final_send"):
            arrived(half_in.at[layer, p], h_recv.at[layer, p])
            for step in range(1, nx):
                b = chip(step)
                both_cores = pbuf[layer, p, c, b].astype(F32) + half_in[layer, p, b].astype(F32)
                fin[0, p, b] = both_cores.astype(BF16)
                go(remote(fin.at[0, p, b], fin.at[1, p, x], f_send.at[p, step], f_recv.at[p, x],
                          peer(step)))

    def final_rows(layer, p):
        with jax.named_scope("final_rows"):
            projected = pbuf[layer, p, c, x].astype(F32) + half_in[layer, p, x].astype(F32)
            for step in range(1, nx):
                b = chip(step)
                arrived(fin.at[1, p, b], f_recv.at[p, b])
                projected = projected + fin[1, p, b].astype(F32)
            value = stream[p, t] + normalize(projected, gains[layer, 1:2, :])
            out[p * prows:(p + 1) * prows, :] = value.astype(out.dtype)

    for layer in range(depth):
        last = layer == depth - 1
        own_pair = s // 2

        @pl.loop(0, PIECES * pairs)
        def _(i):
            p = i // pairs
            k = i % pairs
            attend(layer, p, lax.rem(own_pair + k + (1 if layer == 0 else 0), pairs))
            for later in range(1, PIECES):
                @pl.when(i == later * pairs)
                def _():
                    merge(layer, later - 1)

        drains.append(functools.partial(drain_results, layer))
        if layer == 0:
            @pl.loop(units * depth - (depth - 1), units * depth)
            def _(index):
                project(index)
        merge(layer, PIECES - 1)
        load(3, layer).wait()

        for p in range(PIECES):
            out_project(layer, p)
            if last:
                final_send(layer, p)
            else:
                chip_total(layer, p)
        if not last:
            load(0, layer + 1).wait()
        for p in range(PIECES):
            if last:
                final_rows(layer, p)
            else:
                next_queries(layer, p)
        if not last:
            drains.append(functools.partial(drain_queries, layer + 1))

    finish()


def fused_body(nx, sp, target, source, w_query, w_key, w_value, w_out, gains):
    depth, width, local_width = w_query.shape
    trows, rows = target.shape[0], source.shape[0]
    tp = nx * CORES
    prows = trows // PIECES
    piece_rows = tp * prows
    heads = local_width // HEAD
    units = 2 * nx
    vmem = pltpu.VMEM
    dma = pltpu.SemaphoreType.DMA
    anywhere = pl.BlockSpec(memory_space=pl.ANY)
    whole = pl.BlockSpec(memory_space=pltpu.VMEM)
    results = (depth, PIECES, sp, piece_rows, local_width)
    notes = (depth, PIECES, sp, 2 * heads, 2 * piece_rows)
    return pl.pallas_call(
        functools.partial(fused_kernel, nx, sp, depth),
        out_shape=jax.ShapeDtypeStruct((trows, width), BF16),
        in_specs=[anywhere] * 6 + [whole],
        out_specs=whole,
        scratch_shapes=[
            vmem((tp, trows, width), BF16),
            vmem((units, 2, rows // 2, width), BF16),
            vmem(w_query.shape, BF16),
            vmem(w_key.shape, BF16),
            vmem(w_value.shape, BF16),
            vmem(w_out.shape, BF16),
            vmem((depth, units * rows, local_width), BF16),
            vmem((depth, local_width, units * rows), BF16),
            vmem((PIECES, tp, prows, width), F32),
            vmem((PIECES, tp, prows, width), BF16),
            vmem(results, BF16),
            vmem(results, BF16),
            vmem(results, BF16),
            vmem(notes, F32),
            vmem(notes, F32),
            vmem(results[:2] + results[3:], BF16),
            vmem(notes[:2] + notes[3:], F32),
            vmem((piece_rows, local_width), BF16),
            vmem((depth, PIECES, CORES, nx, prows, width), BF16),
            vmem((depth, PIECES, nx, prows, width), BF16),
            vmem((depth, PIECES, nx, CORES, nx, prows, width), BF16),
            vmem((2, PIECES, nx, prows, width), BF16),
            dma((3,)), dma((4, depth)),
            dma((nx,)), dma((tp,)), dma((nx,)),
            dma((2,)), dma((nx, 4)), dma((units, 4)), dma((units, 2)),
            dma((depth, PIECES, sp)), dma((depth, PIECES, sp)), dma((depth, PIECES)),
            dma((depth, PIECES, sp)), dma((depth, PIECES, sp)),
            dma((depth, PIECES, sp)), dma((depth, PIECES, sp)),
            dma((depth, PIECES)), dma((depth, PIECES)),
            dma((depth, PIECES)), dma((depth, PIECES)),
            dma((depth, PIECES, nx)), dma((depth, PIECES)), dma((depth, PIECES, nx)),
            dma((depth, PIECES, nx)), dma((depth, PIECES, nx)),
            dma((PIECES, nx)), dma((PIECES, nx)),
        ],
        compiler_params=pltpu.CompilerParams(
            collective_id=0, has_side_effects=True, vmem_limit_bytes=60 * 1024 * 1024),
    )(target, source, w_query, w_key, w_value, w_out, gains)


def split_heads(row_block):
    return row_block.reshape(row_block.shape[0], row_block.shape[1] // HEAD, HEAD)


def body(target, source, w_query, w_key, w_value, w_out, gains):
    local_width = w_query.shape[2]
    score_scale = HEAD ** (-0.5)
    depth = w_query.shape[0]
    project_shard_part = lax.all_gather(source, "tp", axis=0, tiled=True)
    layer_parts = [
        jnp.stack(
            [
                jnp.dot(project_shard_part, w_key[level], preferred_element_type=jnp.float32),
                jnp.dot(project_shard_part, w_value[level], preferred_element_type=jnp.float32),
            ]
        )
        for level in range(depth)
    ]
    projected_source = jnp.stack(layer_parts).astype(jnp.bfloat16)
    stream = target.astype(jnp.float32)
    for layer_index in range(depth):
        normed = normalize(stream, gains[layer_index, 0]).astype(jnp.bfloat16)
        query_weight = w_query[layer_index]
        queries = jnp.dot(
            lax.all_gather(normed, "tp", axis=0, tiled=True),
            query_weight,
            preferred_element_type=jnp.float32,
        ).astype(jnp.bfloat16)
        row_count = queries.shape[0]
        keys_here = projected_source[layer_index, 0]
        values_here = projected_source[layer_index, 1]
        every_query = lax.all_gather(queries, "sp", axis=0, tiled=True)
        scores = (
            jnp.einsum(
                "qhd,khd->hqk",
                split_heads(every_query),
                split_heads(keys_here),
                preferred_element_type=jnp.float32,
            )
            * score_scale
        )
        row_peak = lax.pmax(jnp.max(scores, axis=2), "sp")
        weights = jnp.exp(scores - row_peak[:, :, None])
        local_summed = jnp.einsum(
            "hqk,khd->hqd",
            weights.astype(jnp.bfloat16),
            split_heads(values_here),
            preferred_element_type=jnp.float32,
        )
        summed, row_total = (
            lax.psum_scatter(
                local_summed.astype(jnp.bfloat16), "sp", scatter_dimension=1, tiled=True
            ).astype(jnp.float32),
            lax.psum_scatter(
                jnp.sum(weights, axis=2).astype(jnp.bfloat16), "sp", scatter_dimension=1, tiled=True
            ).astype(jnp.float32),
        )
        heads_out = summed / row_total[:, :, None]
        attended = (
            jnp.transpose(heads_out, (1, 0, 2)).reshape(row_count, local_width).astype(jnp.bfloat16)
        )
        out_weight = w_out[layer_index]
        projected = lax.psum_scatter(
            jnp.dot(attended, out_weight, preferred_element_type=jnp.float32).astype(jnp.bfloat16),
            "tp",
            scatter_dimension=0,
            tiled=True,
        ).astype(jnp.float32)
        stream = stream + normalize(projected, gains[layer_index, 1])
    return stream.astype(jnp.bfloat16)


def solution(mesh):
    in_specs = (
        P(("grp", "sp", "tp"), None),
        P(("grp", "sp", "tp"), None),
        P(None, None, "tp"),
        P(None, None, "tp"),
        P(None, None, "tp"),
        P(None, "tp", None),
        P(),
    )
    out_specs = P(("grp", "sp", "tp"), None)
    sp, tp = mesh.shape["sp"], mesh.shape["tp"]

    def run(target, source, w_query, w_key, w_value, w_out, gains):
        trows, rows, local_width = target.shape[0], source.shape[0], w_query.shape[2]
        tiles = (trows % (16 * PIECES) == 0 and tp * trows == PIECES * (HEAD // 2) and rows % 128 == 0
                 and sp % 2 == 0 and sp >= 4
                 and local_width % (4 * HEAD) == 0 and tp % CORES == 0)
        form = functools.partial(fused_body, tp // CORES, sp) if tiles else body
        return form(target, source, w_query, w_key, w_value, w_out, gains)

    return jax.shard_map(run, mesh=mesh, in_specs=in_specs, out_specs=out_specs, check_vma=False)
```

time: 96.5 us -> 94.7 us (0.981)
  Pallas kernels: 94.8 us -> 92.9 us
    pallas_call x1, Pallas kernels: 94.8 us -> 92.9 us  [fused_body(): pl.pallas_call(functools.partial(fused_kernel, nx, sp, depth), out_shape=...]
where the time goes in v1:
time: 94.7 us; the launch traced here: 94.5 us
  Pallas kernels  92.9 us (98%)
  local copies, waits for them, and re-layouts  1.57 us (2%)
    pallas_call x1, Pallas kernels, fused_body(): pl.pallas_call(functools.partial(fused_kernel, nx, sp, depth), out_shape=...  92.9 us

profile of v1, /device:TPU:0, one launch (start us, length us, event | category | flops | bytes accessed | tf_op | source)
XLA Modules:
  0.0 94.5 jit_solution(5280141510108492063)
XLA Ops:
  0.0 92.9 %shard_map.73 = bf16[32,2048]{1,0:T(8,128)(2,1)} custom-call(bf16[32,2048]{1,0:T(8,128)(2,1)} %target.1, bf16[256,2048]{1,0:T(8,128)(2,1)} %source.1, bf16[2,2048,512]{2,1,0:T(8,128)(2,1)} %w_query.1, bf16[2,2048,512]{2,1,0:T(8,128)(2,1)} %w_key.1, bf16[2,2048,512]{2,1,0:T(8,128)(2,1)} %w_value.1, bf16[2,512,2048]{2,1,0:T(8,128)(2,1)} %w_out.1, ...), custom_call_target="tpu_custom_call" | custom-call | tf_op jit(solution)/shard_map/pallas_call | solution.py:521
  92.9 1.6 %copy.9 = bf16[32,2048]{1,0:T(8,128)(2,1)} copy(bf16[32,2048]{1,0:T(8,128)(2,1)} %shard_map.73) | data formatting | bytes 262144

commit v2 on v1

--- a/solution.py
+++ b/solution.py
@@ -11,6 +11,7 @@
 HEAD = 128
 CORES = 2
 PIECES = 2
+MERGED = (2, 2)
 
 
 EPS = 1e-06
@@ -32,10 +33,9 @@
     nx, sp, depth,
     target, source, w_query, w_key, w_value, w_out, gains, out,
     tbuf, sbuf, wq, wk, wv, wo, keys, values, stream, normed, qbuf,
-    osend, orecv, ssend, srecv, orelay, srelay, attended, pbuf, half_in, chip_sum, fin,
-    local_sem, weight_sem, t_send, t_recv, t_fsend, s_psend, s_send, s_recv, s_fsend,
-    q_send, q_recv, q_fsend, o_send, o_recv, e_send, e_recv, or_recv, er_recv,
-    h_send, h_recv, c_send, c_psend, c_fsend, c_recv, c_frecv, f_send, f_recv,
+    osend, orecv, ssend, srecv, orelay, srelay, attended, pbuf, half_in, chip_sum, fin, ledger,
+    local_sem, weight_sem, send_sem, t_recv, s_recv, p_recv, r_recv, first_recv, q_recv,
+    o_recv, m_recv, h_recv, c_recv, d_recv, f_recv,
 ):
     s = lax.axis_index("sp")
     t = lax.axis_index("tp")
@@ -74,20 +74,30 @@
             device_id=device, device_id_type=MESH,
         )
 
-    def arrived(dst, recv_sem):
-        remote(dst, dst, t_send.at[0], recv_sem, partner).wait_recv()
+    def arrived(sem, *shapes):
+        total = sum(math.prod(shape) * size for shape, size in shapes)
+        block = ledger.at[pl.ds(0, total // math.prod(ledger.shape[1:]) // 4)]
+        pltpu.make_async_copy(block, block, sem).wait()
+
+    target_rows = (tbuf.shape[1:], 2)
+    source_part = (sbuf.shape[2:], 2)
+    result_block = (osend.shape[3:], 2)
+    stats_block = (ssend.shape[3:], 4)
+    sum_block = (half_in.shape[3:], 2)
+    chip_rows = (half_in.shape[2:], 2)
+    weight_block = (wk.shape[1:], 2)
 
     own_target = pltpu.make_async_copy(target, tbuf.at[t], local_sem.at[0])
     own_source = [
         pltpu.make_async_copy(
-            source.at[pl.ds(part * half, half)], sbuf.at[0, part], local_sem.at[1 + part])
+            source.at[pl.ds(part * half, half)], sbuf.at[0, part], local_sem.at[1])
         for part in range(2)
     ]
 
     def load(kind, level):
         pair = ((w_query, wq), (w_key, wk), (w_value, wv), (w_out, wo))[kind]
         return pltpu.make_async_copy(
-            pair[0].at[level], pair[1].at[level], weight_sem.at[kind, level])
+            pair[0].at[level], pair[1].at[level], weight_sem.at[(0, 1, 1, 2)[kind], level])
 
     own_target.start()
     for copy in own_source:
@@ -105,32 +115,28 @@
     with jax.named_scope("barrier"):
         pl.semaphore_wait(barrier, 1 + (nx - 1) + (sp - 1))
 
-    sends = []
-
-    drains = []
-
-    def finish():
-        for drain in drains:
-            drain()
-        for copy in sends:
-            copy.wait_send()
-
-    def go(copy):
+    SOURCE, LINE, ROW = range(3)
+    sent = {SOURCE: [], LINE: [], ROW: []}
+
+    def go(copy, kind, shape):
         copy.start()
-        sends.append(copy)
+        sent[kind].append(shape)
 
     for step in range(1, nx):
-        go(remote(target, tbuf.at[t], t_send.at[step], t_recv.at[t], peer(step)))
-    go(remote(target, tbuf.at[t], t_send.at[0], t_recv.at[t], partner))
+        go(remote(target, tbuf.at[t], send_sem.at[SOURCE], t_recv.at[step], peer(step)),
+           SOURCE, target_rows)
+    go(remote(target, tbuf.at[t], send_sem.at[SOURCE], t_recv.at[0], partner), SOURCE, target_rows)
     for part in range(2):
         block = source.at[pl.ds(part * half, half)]
         for piece in range(2):
             span = pl.ds(piece * (half // 2), half // 2)
             for step in range(1, nx):
                 unit = 2 * (nx - step) + part
-                go(remote(block.at[span], sbuf.at[unit, 0, span], s_send.at[step, 2 * part + piece],
-                          s_recv.at[unit, piece], peer(step)))
-        go(remote(block, sbuf.at[1, part], s_psend.at[part], s_recv.at[1, part], partner))
+                go(remote(block.at[span], sbuf.at[unit, 0, span], send_sem.at[SOURCE],
+                          s_recv.at[unit - 2, piece], peer(step)),
+                   SOURCE, ((half // 2, width), 2))
+        go(remote(block, sbuf.at[1, part], send_sem.at[SOURCE], p_recv.at[0], partner),
+           SOURCE, source_part)
 
     def project(index):
         unit = index // depth
@@ -146,82 +152,79 @@
     def far_pair(j):
         return jnp.logical_and(edge, j == mirror)
 
-    def query_copy(level, p, step):
-        return remote(qbuf.at[level, p, s], qbuf.at[level, p, s], q_send.at[level, p, step],
-                      q_recv.at[level, p, s], {"sp": lax.rem(s + step, sp)})
-
-    def query_relay(level, p):
-        return remote(qbuf.at[level, p, relay_to], qbuf.at[level, p, relay_to],
-                      q_fsend.at[level, p], q_recv.at[level, p, relay_to], {"sp": relay_from})
-
-    def each_query(level, p, act):
-        for step in range(1, sp):
-            copy = query_copy(level, p, step)
-            if level == 0:
-                act(copy)
-            else:
-                @pl.when(jnp.logical_not(far_pair(lax.rem(s + step, sp))))
-                def _():
-                    act(copy)
+    def query_copy(level, p, j):
+        sem = first_recv.at[0] if level == 0 else q_recv.at[level - 1, p, s]
+        return remote(qbuf.at[level, p, s], qbuf.at[level, p, s], send_sem.at[LINE], sem, {"sp": j})
+
+    def forward(level, p):
+        @pl.when(relays)
+        def _():
+            arrived(q_recv.at[level - 1, p, relay_to], result_block)
+            block = qbuf.at[level, p, relay_to]
+            remote(block, block, send_sem.at[LINE], q_recv.at[level - 1, p, relay_to],
+                   {"sp": relay_from}).start()
 
     def send_queries(level, p):
-        each_query(level, p, lambda copy: copy.start())
-
-    def drain_queries(level):
-        for p in range(PIECES):
-            each_query(level, p, lambda copy: copy.wait_send())
-            if level > 0:
-                @pl.when(relays)
-                def _():
-                    query_relay(level, p).wait_send()
+        for distance in range(sp - 1 if level == 0 else sp - 2, 0, -1):
+            @pl.when(s + distance < sp)
+            def _():
+                query_copy(level, p, lax.rem(s + distance, sp)).start()
+
+            @pl.when(s >= distance)
+            def _():
+                query_copy(level, p, lax.rem(s + sp - distance, sp)).start()
+
+    def drain_line():
+        def drain(queries):
+            blocks = PIECES * ((depth + 1) * (sp - 1) + (depth - 1) * queries)
+            arrived(send_sem.at[LINE], *([result_block] * blocks),
+                    *([stats_block] * (depth * PIECES * (sp - 1))))
+
+        @pl.when(edge)
+        def _():
+            drain(sp - 2)
+
+        @pl.when(relays)
+        def _():
+            drain(sp)
+
+        if sp > 4:
+            @pl.when(jnp.logical_not(jnp.logical_or(edge, relays)))
+            def _():
+                drain(sp - 1)
+
+    def merged(level, p):
+        return p < MERGED[min(level, 1)]
 
     def result_copies(level, p, j):
         return (
-            remote(osend.at[level, p, j], orecv.at[level, p, s], o_send.at[level, p, j],
-                   o_recv.at[level, p, s], {"sp": j}),
-            remote(ssend.at[level, p, j], srecv.at[level, p, s], e_send.at[level, p, j],
-                   e_recv.at[level, p, s], {"sp": j}),
+            remote(osend.at[level, p, j], orecv.at[level, p, s], send_sem.at[LINE],
+                   o_recv.at[level, p], {"sp": j}),
+            remote(ssend.at[level, p, j], srecv.at[level, p, s], send_sem.at[LINE],
+                   o_recv.at[level, p], {"sp": j}),
         )
 
     def relay_copies(level, p, j):
         return (
-            remote(osend.at[level, p, j], orelay.at[level, p], o_send.at[level, p, j],
-                   or_recv.at[level, p], {"sp": via}),
-            remote(ssend.at[level, p, j], srelay.at[level, p], e_send.at[level, p, j],
-                   er_recv.at[level, p], {"sp": via}),
-        )
-
-    def drain_results(level):
-        for p in range(PIECES):
-            for step in range(1, sp):
-                for copy in result_copies(level, p, lax.rem(s + step, sp)):
-                    copy.wait_send()
-
-    def target_relay(step):
-        slot = chip(step) * CORES + c
-        return remote(tbuf.at[slot], tbuf.at[slot], t_fsend.at[step], t_recv.at[slot], partner)
+            remote(osend.at[level, p, j], orelay.at[level, p], send_sem.at[LINE],
+                   m_recv.at[level, p], {"sp": via}),
+            remote(ssend.at[level, p, j], srelay.at[level, p], send_sem.at[LINE],
+                   m_recv.at[level, p], {"sp": via}),
+        )
 
     def source_relay(unit, piece):
         span = pl.ds(piece * (half // 2), half // 2)
-        return remote(sbuf.at[unit, 0, span], sbuf.at[unit, 1, span], s_fsend.at[unit, piece],
-                      s_recv.at[unit, 2 + piece], partner)
-
-    def drain_relays():
-        for step in range(1, nx):
-            target_relay(step).wait_send()
-        for unit in range(2, units):
-            for piece in range(2):
-                source_relay(unit, piece).wait_send()
+        return remote(sbuf.at[unit, 0, span], sbuf.at[unit, 1, span], send_sem.at[SOURCE],
+                      r_recv.at[unit - 2], partner)
 
     def first_queries():
         own_target.wait()
         for step in range(1, nx):
             slot = chip(step) * CORES + c
-            arrived(tbuf.at[slot], t_recv.at[slot])
-            target_relay(step).start()
-        for step in range(nx):
-            slot = chip(step) * CORES + partner_c
-            arrived(tbuf.at[slot], t_recv.at[slot])
+            arrived(t_recv.at[step], target_rows)
+            go(remote(tbuf.at[slot], tbuf.at[slot], send_sem.at[SOURCE], t_recv.at[0], partner),
+               SOURCE, target_rows)
+        arrived(t_recv.at[0], *([target_rows] * nx))
 
         @pl.loop(0, tp)
         def _(block):
@@ -245,8 +248,9 @@
             empty = jnp.concatenate([lowest, jnp.zeros_like(lowest)], axis=0)
             for level in range(depth):
                 for p in range(PIECES):
-                    orecv[level, p, mirror] = jnp.zeros((piece_rows, local_width), BF16)
-                    srecv[level, p, mirror] = empty
+                    if merged(level, p):
+                        orecv[level, p, mirror] = jnp.zeros((piece_rows, local_width), BF16)
+                        srecv[level, p, mirror] = empty
 
     @pl.loop(0, units * depth - (depth - 1))
     def _(index):
@@ -255,10 +259,8 @@
 
         @pl.when(index == 0)
         def _():
-            for copy in own_source:
-                copy.wait()
-            load(1, 0).wait()
-            load(2, 0).wait()
+            arrived(local_sem.at[1], source_part, source_part)
+            arrived(weight_sem.at[1, 0], weight_block, weight_block)
             load(0, 0).start()
             for later in range(1, depth):
                 load(1, later).start()
@@ -271,30 +273,26 @@
         for later in range(1, depth):
             @pl.when(index == later)
             def _():
-                load(1, later).wait()
-                load(2, later).wait()
+                arrived(weight_sem.at[1, later], weight_block, weight_block)
 
         @pl.when(index == depth)
         def _():
             with jax.named_scope("first_queries"):
                 first_queries()
-            for part in range(2):
-                arrived(sbuf.at[1, part], s_recv.at[1, part])
+            arrived(p_recv.at[0], source_part, source_part)
 
         @pl.when(jnp.logical_and(unit >= 2, level == 0))
         def _():
             with jax.named_scope("wait_remote"):
                 for piece in range(2):
-                    span = pl.ds(piece * (half // 2), half // 2)
-                    arrived(sbuf.at[unit, 0, span], s_recv.at[unit, piece])
+                    arrived(s_recv.at[unit - 2, piece], ((half // 2, width), 2))
                     source_relay(unit, piece).start()
-                for piece in range(2):
-                    span = pl.ds(piece * (half // 2), half // 2)
-                    arrived(sbuf.at[unit, 1, span], s_recv.at[unit, 2 + piece])
+                arrived(r_recv.at[unit - 2], source_part)
 
         project(index)
 
-    drains += [drain_relays, functools.partial(drain_queries, 0)]
+    sent[SOURCE] += [source_part] * (units - 2)
+    arrived(first_recv.at[0], *([result_block] * (PIECES * (sp - 1))))
 
     def columns(parts):
         stacked = jnp.concatenate(parts, axis=0)
@@ -311,8 +309,7 @@
         @pl.when(relays)
         def _():
           with jax.named_scope("merge"):
-            arrived(orelay.at[layer, p], or_recv.at[layer, p])
-            arrived(srelay.at[layer, p], er_recv.at[layer, p])
+            arrived(m_recv.at[layer, p], result_block, stats_block)
             mine, theirs = ssend[layer, p, relay_to], srelay[layer, p]
             top = jnp.maximum(mine[0:heads], theirs[0:heads])
             share = [jnp.exp2(one[0:heads] - top) for one in (mine, theirs)]
@@ -330,16 +327,13 @@
         first = 2 * pair
         for member in range(2):
             j = first + member
-
-            @pl.when(j != s)
-            def _():
-                with jax.named_scope("wait_q"):
-                    arrived(qbuf.at[layer, p, j], q_recv.at[layer, p, j])
-
             if layer > 0:
-                @pl.when(jnp.logical_and(relays, j == relay_to))
+                taken = jnp.logical_or(j == s, jnp.logical_and(relays, j == relay_to))
+
+                @pl.when(jnp.logical_not(taken))
                 def _():
-                    query_relay(layer, p).start()
+                    with jax.named_scope("wait_q"):
+                        arrived(q_recv.at[layer - 1, p, j], result_block)
 
         with jax.named_scope("attend"):
             q = qbuf[layer, p, pl.ds(first, 2)].reshape(2 * piece_rows, local_width)
@@ -369,27 +363,31 @@
                 orecv[layer, p, s] = osend[layer, p, s]
                 srecv[layer, p, s] = ssend[layer, p, s]
 
-            @pl.when(far_pair(j))
+            aside = jnp.logical_and(far_pair(j), merged(layer, p))
+            held = jnp.logical_and(jnp.logical_and(relays, j == relay_to), merged(layer, p))
+
+            @pl.when(aside)
             def _():
                 for copy in relay_copies(layer, p, j):
                     copy.start()
 
-            held = jnp.logical_or(far_pair(j), jnp.logical_and(relays, j == relay_to))
-
-            @pl.when(jnp.logical_not(jnp.logical_or(held, j == s)))
+            @pl.when(jnp.logical_not(functools.reduce(jnp.logical_or, (j == s, aside, held))))
             def _():
                 for copy in result_copies(layer, p, j):
                     copy.start()
 
     def out_project(layer, p):
         with jax.named_scope("wait_o"):
-            for step in range(1, sp):
-                j = lax.rem(s + step, sp)
-
-                @pl.when(jnp.logical_not(far_pair(j)))
+            if merged(layer, p):
+                @pl.when(edge)
                 def _():
-                    arrived(orecv.at[layer, p, j], o_recv.at[layer, p, j])
-                    arrived(srecv.at[layer, p, j], e_recv.at[layer, p, j])
+                    arrived(o_recv.at[layer, p], *([result_block, stats_block] * (sp - 2)))
+
+                @pl.when(jnp.logical_not(edge))
+                def _():
+                    arrived(o_recv.at[layer, p], *([result_block, stats_block] * (sp - 1)))
+            else:
+                arrived(o_recv.at[layer, p], *([result_block, stats_block] * (sp - 1)))
         with jax.named_scope("combine_out"):
             stats = [srecv[layer, p, j] for j in range(sp)]
             top = functools.reduce(jnp.maximum, [one[0:heads] for one in stats])
@@ -407,30 +405,29 @@
                     for core in range(CORES):
                         at = (b * CORES + core) * prows
                         pbuf[layer, p, core, b, :, span] = part[at:at + prows]
-            go(remote(pbuf.at[layer, p, partner_c], half_in.at[layer, p], h_send.at[layer, p],
-                      h_recv.at[layer, p], partner))
+            go(remote(pbuf.at[layer, p, partner_c], half_in.at[layer, p], send_sem.at[ROW],
+                      h_recv.at[layer, p], partner), ROW, chip_rows)
 
     def chip_total(layer, p):
         with jax.named_scope("chip_total"):
-            arrived(half_in.at[layer, p], h_recv.at[layer, p])
+            arrived(h_recv.at[layer, p], chip_rows)
             for b in range(nx):
                 both_cores = pbuf[layer, p, c, b].astype(F32) + half_in[layer, p, b].astype(F32)
                 chip_sum[layer, p, x, c, b] = both_cores.astype(BF16)
             own = chip_sum.at[layer, p, x, c]
             for step in range(1, nx):
-                go(remote(own, own, c_send.at[layer, p, step], c_recv.at[layer, p, x], peer(step)))
-            go(remote(own, own, c_psend.at[layer, p], c_frecv.at[layer, p, x], partner))
+                go(remote(own, own, send_sem.at[ROW], c_recv.at[layer, p, nx - step - 1], peer(step)),
+                   ROW, chip_rows)
+            go(remote(own, own, send_sem.at[ROW], d_recv.at[layer, p], partner), ROW, chip_rows)
 
     def next_queries(layer, p):
         with jax.named_scope("xwait"):
             for step in range(1, nx):
                 a = chip(step)
                 other = chip_sum.at[layer, p, a, c]
-                arrived(other, c_recv.at[layer, p, a])
-                go(remote(other, other, c_fsend.at[layer, p, step], c_frecv.at[layer, p, a], partner))
-            for step in range(nx):
-                a = chip(step)
-                arrived(chip_sum.at[layer, p, a, partner_c], c_frecv.at[layer, p, a])
+                arrived(c_recv.at[layer, p, step - 1], chip_rows)
+                go(remote(other, other, send_sem.at[ROW], d_recv.at[layer, p], partner), ROW, chip_rows)
+            arrived(d_recv.at[layer, p], *([chip_rows] * nx))
         with jax.named_scope("norm_q"):
             for block in range(tp):
                 projected = sum(
@@ -445,20 +442,20 @@
 
     def final_send(layer, p):
         with jax.named_scope("final_send"):
-            arrived(half_in.at[layer, p], h_recv.at[layer, p])
+            arrived(h_recv.at[layer, p], chip_rows)
             for step in range(1, nx):
                 b = chip(step)
                 both_cores = pbuf[layer, p, c, b].astype(F32) + half_in[layer, p, b].astype(F32)
                 fin[0, p, b] = both_cores.astype(BF16)
-                go(remote(fin.at[0, p, b], fin.at[1, p, x], f_send.at[p, step], f_recv.at[p, x],
-                          peer(step)))
+                go(remote(fin.at[0, p, b], fin.at[1, p, x], send_sem.at[ROW],
+                          f_recv.at[p, nx - step - 1], peer(step)), ROW, sum_block)
 
     def final_rows(layer, p):
         with jax.named_scope("final_rows"):
             projected = pbuf[layer, p, c, x].astype(F32) + half_in[layer, p, x].astype(F32)
             for step in range(1, nx):
                 b = chip(step)
-                arrived(fin.at[1, p, b], f_recv.at[p, b])
+                arrived(f_recv.at[p, step - 1], sum_block)
                 projected = projected + fin[1, p, b].astype(F32)
             value = stream[p, t] + normalize(projected, gains[layer, 1:2, :])
             out[p * prows:(p + 1) * prows, :] = value.astype(out.dtype)
@@ -466,23 +463,33 @@
     for layer in range(depth):
         last = layer == depth - 1
         own_pair = s // 2
-
-        @pl.loop(0, PIECES * pairs)
+        count = PIECES * pairs
+
+        @pl.loop(0, count)
         def _(i):
-            p = i // pairs
-            k = i % pairs
-            attend(layer, p, lax.rem(own_pair + k + (1 if layer == 0 else 0), pairs))
-            for later in range(1, PIECES):
-                @pl.when(i == later * pairs)
-                def _():
-                    merge(layer, later - 1)
-
-        drains.append(functools.partial(drain_results, layer))
+            if layer == 0:
+                p, k = i // pairs, i % pairs + 1
+            else:
+                p, k = i % PIECES, i // PIECES
+                for later in range(PIECES):
+                    @pl.when(i == (0 if later == 0 else count - PIECES + later))
+                    def _():
+                        forward(layer, later)
+            attend(layer, p, lax.rem(own_pair + k, pairs))
+            if layer == 0:
+                for later in range(1, PIECES):
+                    if merged(layer, later - 1):
+                        @pl.when(i == later * pairs)
+                        def _():
+                            merge(layer, later - 1)
+
         if layer == 0:
             @pl.loop(units * depth - (depth - 1), units * depth)
             def _(index):
                 project(index)
-        merge(layer, PIECES - 1)
+        for p in range(PIECES):
+            if merged(layer, p) and (layer > 0 or p == PIECES - 1):
+                merge(layer, p)
         load(3, layer).wait()
 
         for p in range(PIECES):
@@ -498,10 +505,11 @@
                 final_rows(layer, p)
             else:
                 next_queries(layer, p)
-        if not last:
-            drains.append(functools.partial(drain_queries, layer + 1))
-
-    finish()
+
+    with jax.named_scope("finish"):
+        drain_line()
+        for kind in (SOURCE, ROW):
+            arrived(send_sem.at[kind], *sent[kind])
 
 
 def fused_body(nx, sp, target, source, w_query, w_key, w_value, w_out, gains):
@@ -546,17 +554,11 @@
             vmem((depth, PIECES, nx, prows, width), BF16),
             vmem((depth, PIECES, nx, CORES, nx, prows, width), BF16),
             vmem((2, PIECES, nx, prows, width), BF16),
-            dma((3,)), dma((4, depth)),
-            dma((nx,)), dma((tp,)), dma((nx,)),
-            dma((2,)), dma((nx, 4)), dma((units, 4)), dma((units, 2)),
-            dma((depth, PIECES, sp)), dma((depth, PIECES, sp)), dma((depth, PIECES)),
-            dma((depth, PIECES, sp)), dma((depth, PIECES, sp)),
-            dma((depth, PIECES, sp)), dma((depth, PIECES, sp)),
-            dma((depth, PIECES)), dma((depth, PIECES)),
-            dma((depth, PIECES)), dma((depth, PIECES)),
-            dma((depth, PIECES, nx)), dma((depth, PIECES)), dma((depth, PIECES, nx)),
-            dma((depth, PIECES, nx)), dma((depth, PIECES, nx)),
-            dma((PIECES, nx)), dma((PIECES, nx)),
+            vmem((1024, 8, 128), F32),
+            dma((2,)), dma((3, depth)), dma((3,)), dma((nx,)),
+            dma((units - 2, 2)), dma((1,)), dma((units - 2,)), dma((1,)), dma((depth - 1, PIECES, sp)),
+            dma((depth, PIECES)), dma((depth, PIECES)), dma((depth, PIECES)),
+            dma((depth - 1, PIECES, nx - 1)), dma((depth - 1, PIECES)), dma((PIECES, nx - 1)),
         ],
         compiler_params=pltpu.CompilerParams(
             collective_id=0, has_side_effects=True, vmem_limit_bytes=60 * 1024 * 1024),
@@ -651,7 +653,7 @@
     def run(target, source, w_query, w_key, w_value, w_out, gains):
         trows, rows, local_width = target.shape[0], source.shape[0], w_query.shape[2]
         tiles = (trows % (16 * PIECES) == 0 and tp * trows == PIECES * (HEAD // 2) and rows % 128 == 0
-                 and sp % 2 == 0 and sp >= 4
+                 and sp % 2 == 0 and sp >= 4 and w_query.shape[0] > 1 and tp > CORES
                  and local_width % (4 * HEAD) == 0 and tp % CORES == 0)
         form = functools.partial(fused_body, tp // CORES, sp) if tiles else body
         return form(target, source, w_query, w_key, w_value, w_out, gains)

time: 94.7 us -> 85.2 us (0.90)
  Pallas kernels: 92.9 us -> 83.4 us
    pallas_call x1, Pallas kernels: 92.9 us -> 83.4 us  [fused_body(): pl.pallas_call(functools.partial(fused_kernel, nx, sp, depth), out_shape=...]
where the time goes in v2:
time: 85.2 us; the launch traced here: 85 us
  Pallas kernels  83.4 us (98%)
  local copies, waits for them, and re-layouts  1.57 us (2%)
    pallas_call x1, Pallas kernels, fused_body(): pl.pallas_call(functools.partial(fused_kernel, nx, sp, depth), out_shape=...  83.4 us

profile of v2, /device:TPU:0, one launch (start us, length us, event | category | flops | bytes accessed | tf_op | source)
XLA Modules:
  0.0 85.0 jit_solution(5659114027656573310)
XLA Ops:
  0.0 83.4 %shard_map.73 = bf16[32,2048]{1,0:T(8,128)(2,1)} custom-call(bf16[32,2048]{1,0:T(8,128)(2,1)} %target.1, bf16[256,2048]{1,0:T(8,128)(2,1)} %source.1, bf16[2,2048,512]{2,1,0:T(8,128)(2,1)} %w_query.1, bf16[2,2048,512]{2,1,0:T(8,128)(2,1)} %w_key.1, bf16[2,2048,512]{2,1,0:T(8,128)(2,1)} %w_value.1, bf16[2,512,2048]{2,1,0:T(8,128)(2,1)} %w_out.1, ...), custom_call_target="tpu_custom_call" | custom-call | tf_op jit(solution)/shard_map/pallas_call | solution.py:529
  83.4 1.6 %copy.9 = bf16[32,2048]{1,0:T(8,128)(2,1)} copy(bf16[32,2048]{1,0:T(8,128)(2,1)} %shard_map.73) | data formatting | bytes 262144

commit v3 on v2

--- a/solution.py
+++ b/solution.py
@@ -11,13 +11,12 @@
 HEAD = 128
 CORES = 2
 PIECES = 2
-MERGED = (2, 2)
+VMEM_KIB = 54100
 
 
 EPS = 1e-06
 MESH = pl.DeviceIdType.MESH
 F32 = jnp.float32
-LOWEST = -1e30
 BF16 = jnp.bfloat16
 
 
@@ -31,9 +30,9 @@
 
 def fused_kernel(
     nx, sp, depth,
-    target, source, w_query, w_key, w_value, w_out, gains, out,
+    target, source, w_query, w_key, w_value, w_out, gain_rows, out,
     tbuf, sbuf, wq, wk, wv, wo, keys, values, stream, normed, qbuf,
-    osend, orecv, ssend, srecv, orelay, srelay, attended, pbuf, half_in, chip_sum, fin, ledger,
+    osend, orecv, ssend, srecv, orelay, srelay, attended, pbuf, half_in, chip_sum, fin, ledger, gains,
     local_sem, weight_sem, send_sem, t_recv, s_recv, p_recv, r_recv, first_recv, q_recv,
     o_recv, m_recv, h_recv, c_recv, d_recv, f_recv,
 ):
@@ -56,11 +55,11 @@
 
     pairs = sp // 2
     edge = jnp.logical_or(s == 0, s == sp - 1)
-    mirror = sp - 1 - s
-    relays = jnp.logical_or(s == 1, s == sp - 2)
-    relay_from = jnp.where(s == 1, 0, sp - 1)
-    relay_to = sp - 1 - relay_from
-    via = jnp.where(s == 0, 1, sp - 2)
+    inner = jnp.logical_not(edge)
+    low = s < pairs
+    near = jnp.where(s % 2 == 0, s + 1, s - 1)
+    far_edge = jnp.where(low, sp - 1, 0)
+    far_inner = jnp.where(low, pairs, pairs - 1)
 
     def chip(step):
         return lax.rem(x + step, nx)
@@ -99,7 +98,9 @@
         return pltpu.make_async_copy(
             pair[0].at[level], pair[1].at[level], weight_sem.at[(0, 1, 1, 2)[kind], level])
 
+    own_gains = pltpu.make_async_copy(gain_rows, gains, local_sem.at[2])
     own_target.start()
+    own_gains.start()
     for copy in own_source:
         copy.start()
     load(1, 0).start()
@@ -115,6 +116,7 @@
     with jax.named_scope("barrier"):
         pl.semaphore_wait(barrier, 1 + (nx - 1) + (sp - 1))
 
+    spans = ((0, half // 2), (half // 2, half // 4), (3 * half // 4, half // 8), (7 * half // 8, half // 8))
     SOURCE, LINE, ROW = range(3)
     sent = {SOURCE: [], LINE: [], ROW: []}
 
@@ -128,13 +130,13 @@
     go(remote(target, tbuf.at[t], send_sem.at[SOURCE], t_recv.at[0], partner), SOURCE, target_rows)
     for part in range(2):
         block = source.at[pl.ds(part * half, half)]
-        for piece in range(2):
-            span = pl.ds(piece * (half // 2), half // 2)
+        for piece, (at, size) in enumerate(spans):
+            span = pl.ds(at, size)
             for step in range(1, nx):
                 unit = 2 * (nx - step) + part
                 go(remote(block.at[span], sbuf.at[unit, 0, span], send_sem.at[SOURCE],
                           s_recv.at[unit - 2, piece], peer(step)),
-                   SOURCE, ((half // 2, width), 2))
+                   SOURCE, ((size, width), 2))
         go(remote(block, sbuf.at[1, part], send_sem.at[SOURCE], p_recv.at[0], partner),
            SOURCE, source_part)
 
@@ -147,32 +149,39 @@
             k = jnp.dot(block, wk[level], preferred_element_type=F32)
             keys[level, pl.ds(start, rows), :] = k.astype(BF16)
             v = jnp.dot(block, wv[level], preferred_element_type=F32)
-            values[level, :, pl.ds(start, rows)] = v.T.astype(BF16)
-
-    def far_pair(j):
-        return jnp.logical_and(edge, j == mirror)
-
-    def query_copy(level, p, j):
-        sem = first_recv.at[0] if level == 0 else q_recv.at[level - 1, p, s]
-        return remote(qbuf.at[level, p, s], qbuf.at[level, p, s], send_sem.at[LINE], sem, {"sp": j})
+            values[level, pl.ds(start, rows), :] = v.astype(BF16)
+
+    def project_half(unit, level, part):
+        with jax.named_scope("project_half"):
+            block = sbuf[unit, :, pl.ds(part * (half // 2), half // 2)].reshape(half, width)
+            start = pl.multiple_of(unit * rows + part * half, half)
+            k = jnp.dot(block, wk[level], preferred_element_type=F32)
+            keys[level, pl.ds(start, half), :] = k.astype(BF16)
+            v = jnp.dot(block, wv[level], preferred_element_type=F32)
+            values[level, pl.ds(start, half), :] = v.astype(BF16)
+
+    def query_copy(level, p, block, j):
+        sem = first_recv.at[0] if level == 0 else q_recv.at[level - 1, p, block]
+        rows_of = qbuf.at[level, p, block]
+        return remote(rows_of, rows_of, send_sem.at[LINE], sem, {"sp": j})
 
     def forward(level, p):
-        @pl.when(relays)
-        def _():
-            arrived(q_recv.at[level - 1, p, relay_to], result_block)
-            block = qbuf.at[level, p, relay_to]
-            remote(block, block, send_sem.at[LINE], q_recv.at[level - 1, p, relay_to],
-                   {"sp": relay_from}).start()
+        @pl.when(inner)
+        def _():
+            for block in (far_inner, far_edge):
+                arrived(q_recv.at[level - 1, p, block], result_block)
+                query_copy(level, p, block, near).start()
 
     def send_queries(level, p):
-        for distance in range(sp - 1 if level == 0 else sp - 2, 0, -1):
-            @pl.when(s + distance < sp)
+        if level == 0:
+            query_copy(level, p, s, far_edge).start()
+        query_copy(level, p, s, far_inner).start()
+        if level == 0 or p == 0:
+            query_copy(level, p, s, near).start()
+        else:
+            @pl.when(edge)
             def _():
-                query_copy(level, p, lax.rem(s + distance, sp)).start()
-
-            @pl.when(s >= distance)
-            def _():
-                query_copy(level, p, lax.rem(s + sp - distance, sp)).start()
+                query_copy(level, p, s, near).start()
 
     def drain_line():
         def drain(queries):
@@ -182,43 +191,38 @@
 
         @pl.when(edge)
         def _():
-            drain(sp - 2)
-
-        @pl.when(relays)
-        def _():
-            drain(sp)
-
-        if sp > 4:
-            @pl.when(jnp.logical_not(jnp.logical_or(edge, relays)))
-            def _():
-                drain(sp - 1)
-
-    def merged(level, p):
-        return p < MERGED[min(level, 1)]
-
-    def result_copies(level, p, j):
-        return (
-            remote(osend.at[level, p, j], orecv.at[level, p, s], send_sem.at[LINE],
-                   o_recv.at[level, p], {"sp": j}),
-            remote(ssend.at[level, p, j], srecv.at[level, p, s], send_sem.at[LINE],
-                   o_recv.at[level, p], {"sp": j}),
-        )
-
-    def relay_copies(level, p, j):
-        return (
-            remote(osend.at[level, p, j], orelay.at[level, p], send_sem.at[LINE],
-                   m_recv.at[level, p], {"sp": via}),
-            remote(ssend.at[level, p, j], srelay.at[level, p], send_sem.at[LINE],
-                   m_recv.at[level, p], {"sp": via}),
-        )
+            drain(2)
+
+        @pl.when(inner)
+        def _():
+            drain(4)
+
+    def send_result(level, p, j):
+        remote(osend.at[level, p, j], orecv.at[level, p, s], send_sem.at[LINE],
+               o_recv.at[level, p], {"sp": j}).start()
+        remote(ssend.at[level, p, j], srecv.at[level, p, s], send_sem.at[LINE],
+               o_recv.at[level, p], {"sp": j}).start()
+
+    def send_aside(level, p):
+        for slot, j in enumerate((far_edge, far_inner)):
+            remote(osend.at[level, p, j], orelay.at[level, p, slot], send_sem.at[LINE],
+                   m_recv.at[level, p, slot], {"sp": near}).start()
+            remote(ssend.at[level, p, j], srelay.at[level, p, slot], send_sem.at[LINE],
+                   m_recv.at[level, p, slot], {"sp": near}).start()
 
     def source_relay(unit, piece):
-        span = pl.ds(piece * (half // 2), half // 2)
+        span = pl.ds(*spans[piece])
         return remote(sbuf.at[unit, 0, span], sbuf.at[unit, 1, span], send_sem.at[SOURCE],
-                      r_recv.at[unit - 2], partner)
+                      r_recv.at[unit - 2, min(piece, 1)], partner)
+
+    def relay_pieces(unit, pieces):
+        for piece in pieces:
+            arrived(s_recv.at[unit - 2, piece], ((spans[piece][1], width), 2))
+            source_relay(unit, piece).start()
 
     def first_queries():
         own_target.wait()
+        own_gains.wait()
         for step in range(1, nx):
             slot = chip(step) * CORES + c
             arrived(t_recv.at[step], target_rows)
@@ -241,16 +245,6 @@
         for p in range(PIECES):
             qbuf[0, p, s] = q[p * piece_rows:(p + 1) * piece_rows].astype(BF16)
             send_queries(0, p)
-
-        @pl.when(edge)
-        def _():
-            lowest = jnp.full((heads, 2 * piece_rows), LOWEST, F32)
-            empty = jnp.concatenate([lowest, jnp.zeros_like(lowest)], axis=0)
-            for level in range(depth):
-                for p in range(PIECES):
-                    if merged(level, p):
-                        orecv[level, p, mirror] = jnp.zeros((piece_rows, local_width), BF16)
-                        srecv[level, p, mirror] = empty
 
     @pl.loop(0, units * depth - (depth - 1))
     def _(index):
@@ -284,12 +278,25 @@
         @pl.when(jnp.logical_and(unit >= 2, level == 0))
         def _():
             with jax.named_scope("wait_remote"):
-                for piece in range(2):
-                    arrived(s_recv.at[unit - 2, piece], ((half // 2, width), 2))
-                    source_relay(unit, piece).start()
-                arrived(r_recv.at[unit - 2], source_part)
-
-        project(index)
+                relay_pieces(unit, (0,))
+                arrived(r_recv.at[unit - 2, 0], ((half // 2, width), 2))
+
+            @pl.when(unit == units - 1)
+            def _():
+                project_half(unit, level, 0)
+
+            with jax.named_scope("wait_remote2"):
+                relay_pieces(unit, range(1, len(spans)))
+            with jax.named_scope("wait_relayed"):
+                arrived(r_recv.at[unit - 2, 1], ((half // 2, width), 2))
+
+            @pl.when(unit == units - 1)
+            def _():
+                project_half(unit, level, 1)
+
+        @pl.when(index < (units - 1) * depth)
+        def _():
+            project(index)
 
     sent[SOURCE] += [source_part] * (units - 2)
     arrived(first_recv.at[0], *([result_block] * (PIECES * (sp - 1))))
@@ -306,95 +313,70 @@
             for k, block in enumerate(blocks))
 
     def merge(layer, p):
-        @pl.when(relays)
-        def _():
-          with jax.named_scope("merge"):
-            arrived(m_recv.at[layer, p], result_block, stats_block)
-            mine, theirs = ssend[layer, p, relay_to], srelay[layer, p]
-            top = jnp.maximum(mine[0:heads], theirs[0:heads])
-            share = [jnp.exp2(one[0:heads] - top) for one in (mine, theirs)]
-            total = share[0] * mine[heads:] + share[1] * theirs[heads:]
-            cols = columns(share)
-            blocks = (osend[layer, p, relay_to], orelay[layer, p])
+        @pl.when(inner)
+        def _():
+            for slot, j in enumerate((far_edge, far_inner)):
+                with jax.named_scope("merge_wait"):
+                    arrived(m_recv.at[layer, p, slot], result_block, stats_block)
+                with jax.named_scope("merge"):
+                    mine, theirs = ssend[layer, p, j], srelay[layer, p, slot]
+                    top = jnp.maximum(mine[0:heads], theirs[0:heads])
+                    share = [jnp.exp2(one[0:heads] - top) for one in (mine, theirs)]
+                    total = share[0] * mine[heads:] + share[1] * theirs[heads:]
+                    cols = columns(share)
+                    blocks = (osend[layer, p, j], orelay[layer, p, slot])
+                    for h in range(heads):
+                        osend[layer, p, j, :, h * HEAD:(h + 1) * HEAD] = weighted(
+                            cols, blocks, h).astype(BF16)
+                    ssend[layer, p, j] = jnp.concatenate([top, total], axis=0)
+                    send_result(layer, p, j)
+
+    def head_scores(layer, q, h):
+        cols = slice(h * HEAD, (h + 1) * HEAD)
+        scores = lax.dot_general(
+            q[:, cols], keys[layer, :, cols], (((1,), (1,)), ((), ())), preferred_element_type=F32)
+        return scores, jnp.max(scores, axis=1, keepdims=True) * score_scale
+
+    def attend(layer, p, first, blocks):
+        with jax.named_scope("attend"):
+            count = blocks * piece_rows
+            q = qbuf[layer, p, pl.ds(first, blocks)].reshape(count, local_width)
+            lane = lax.broadcasted_iota(jnp.int32, (count, HEAD), 1)
+            notes = jnp.zeros((count, HEAD), F32)
+            ahead = head_scores(layer, q, 0)
             for h in range(heads):
-                osend[layer, p, relay_to, :, h * HEAD:(h + 1) * HEAD] = weighted(
-                    cols, blocks, h).astype(BF16)
-            ssend[layer, p, relay_to] = jnp.concatenate([top, total], axis=0)
-            for copy in result_copies(layer, p, relay_to):
-                copy.start()
-
-    def attend(layer, p, pair):
-        first = 2 * pair
-        for member in range(2):
-            j = first + member
-            if layer > 0:
-                taken = jnp.logical_or(j == s, jnp.logical_and(relays, j == relay_to))
-
-                @pl.when(jnp.logical_not(taken))
-                def _():
-                    with jax.named_scope("wait_q"):
-                        arrived(q_recv.at[layer - 1, p, j], result_block)
-
-        with jax.named_scope("attend"):
-            q = qbuf[layer, p, pl.ds(first, 2)].reshape(2 * piece_rows, local_width)
-            peaks, totals = [], []
-            for h in range(heads):
+                scores, peak = ahead
+                if h + 1 < heads:
+                    ahead = head_scores(layer, q, h + 1)
                 cols = slice(h * HEAD, (h + 1) * HEAD)
-                scores = lax.dot_general(
-                    keys[layer, :, cols], q[:, cols], (((1,), (1,)), ((), ())),
-                    preferred_element_type=F32)
-                peak = jnp.max(scores, axis=0, keepdims=True) * score_scale
                 weights = jnp.exp2(scores * score_scale - peak)
-                totals.append(jnp.sum(weights, axis=0, keepdims=True))
-                peaks.append(peak)
-                o = jnp.dot(values[layer, cols, :], weights.astype(BF16), preferred_element_type=F32)
-                o = o.T.astype(BF16)
-                for member in range(2):
+                total = jnp.sum(weights, axis=1, keepdims=True)
+                o = jnp.dot(weights.astype(BF16), values[layer, :, cols], preferred_element_type=F32)
+                o = o.astype(BF16)
+                for member in range(blocks):
                     osend[layer, p, first + member, :, cols] = o[member * piece_rows:(member + 1) * piece_rows]
-            stats = jnp.concatenate(peaks + totals, axis=0)
-            ssend[layer, p, first] = stats
-            ssend[layer, p, first + 1] = pltpu.roll(stats, piece_rows, 1)
-
-        for member in (1, 0):
-            j = first + member
-
-            @pl.when(j == s)
-            def _():
-                orecv[layer, p, s] = osend[layer, p, s]
-                srecv[layer, p, s] = ssend[layer, p, s]
-
-            aside = jnp.logical_and(far_pair(j), merged(layer, p))
-            held = jnp.logical_and(jnp.logical_and(relays, j == relay_to), merged(layer, p))
-
-            @pl.when(aside)
-            def _():
-                for copy in relay_copies(layer, p, j):
-                    copy.start()
-
-            @pl.when(jnp.logical_not(functools.reduce(jnp.logical_or, (j == s, aside, held))))
-            def _():
-                for copy in result_copies(layer, p, j):
-                    copy.start()
+                notes = jnp.where(lane == h, peak, notes)
+                notes = jnp.where(lane == heads + h, total, notes)
+            for two in range(blocks // 2):
+                stats = notes[two * HEAD:(two + 1) * HEAD].T[0:2 * heads]
+                ssend[layer, p, first + 2 * two] = stats
+                ssend[layer, p, first + 2 * two + 1] = pltpu.roll(stats, piece_rows, 1)
+
+    def keep_own(layer, p):
+        orecv[layer, p, s] = osend[layer, p, s]
+        srecv[layer, p, s] = ssend[layer, p, s]
 
     def out_project(layer, p):
         with jax.named_scope("wait_o"):
-            if merged(layer, p):
-                @pl.when(edge)
-                def _():
-                    arrived(o_recv.at[layer, p], *([result_block, stats_block] * (sp - 2)))
-
-                @pl.when(jnp.logical_not(edge))
-                def _():
-                    arrived(o_recv.at[layer, p], *([result_block, stats_block] * (sp - 1)))
-            else:
-                arrived(o_recv.at[layer, p], *([result_block, stats_block] * (sp - 1)))
+            arrived(o_recv.at[layer, p], *([result_block, stats_block] * 2))
         with jax.named_scope("combine_out"):
-            stats = [srecv[layer, p, j] for j in range(sp)]
+            origins = (s, near, far_inner)
+            stats = [srecv[layer, p, j] for j in origins]
             top = functools.reduce(jnp.maximum, [one[0:heads] for one in stats])
             share = [jnp.exp2(one[0:heads] - top) for one in stats]
             total = sum(part * one[heads:] for part, one in zip(share, stats))
             cols = columns([part / total for part in share])
-            blocks = [orecv[layer, p, j] for j in range(sp)]
+            blocks = [orecv[layer, p, j] for j in origins]
             for h in range(heads):
                 attended[:, h * HEAD:(h + 1) * HEAD] = weighted(cols, blocks, h).astype(BF16)
             tile = min(512, width)
@@ -463,41 +445,73 @@
     for layer in range(depth):
         last = layer == depth - 1
         own_pair = s // 2
-        count = PIECES * pairs
-
-        @pl.loop(0, count)
-        def _(i):
-            if layer == 0:
-                p, k = i // pairs, i % pairs + 1
-            else:
-                p, k = i % PIECES, i // PIECES
-                for later in range(PIECES):
-                    @pl.when(i == (0 if later == 0 else count - PIECES + later))
-                    def _():
-                        forward(layer, later)
-            attend(layer, p, lax.rem(own_pair + k, pairs))
-            if layer == 0:
-                for later in range(1, PIECES):
-                    if merged(layer, later - 1):
-                        @pl.when(i == later * pairs)
-                        def _():
-                            merge(layer, later - 1)
-
-        if layer == 0:
+        if layer == 1:
             @pl.loop(units * depth - (depth - 1), units * depth)
             def _(index):
                 project(index)
+
+        if layer == 0:
+            @pl.loop(0, 2 * PIECES)
+            def _(i):
+                p, far = i % PIECES, i < PIECES
+                attend(layer, p, jnp.where(far, 2 * (1 - own_pair), 2 * own_pair), 2)
+
+                @pl.when(jnp.logical_and(edge, far))
+                def _():
+                    send_aside(layer, p)
+
+                @pl.when(jnp.logical_not(far))
+                def _():
+                    send_result(layer, p, near)
+                    keep_own(layer, p)
+        else:
+            @pl.loop(0, 2 * PIECES)
+            def _(i):
+                p, close = i // 2, i % 2 == 0
+
+                @pl.when(close)
+                def _():
+                    forward(layer, p)
+
+                    @pl.when(jnp.logical_and(inner, p + 1 < PIECES))
+                    def _():
+                        query_copy(layer, p + 1, s, near).start()
+
+                    with jax.named_scope("wait_near"):
+                        arrived(q_recv.at[layer - 1, p, near], result_block)
+
+                @pl.when(jnp.logical_and(edge, jnp.logical_not(close)))
+                def _():
+                    with jax.named_scope("wait_far"):
+                        for block in (far_inner, far_edge):
+                            arrived(q_recv.at[layer - 1, p, block], result_block)
+
+                attend(layer, p, jnp.where(close, 2 * own_pair, 2 * (1 - own_pair)), 2)
+
+                @pl.when(close)
+                def _():
+                    keep_own(layer, p)
+
+                @pl.when(jnp.logical_and(edge, close))
+                def _():
+                    send_result(layer, p, near)
+
+                @pl.when(jnp.logical_and(inner, i == 2 * PIECES - 2))
+                def _():
+                    for later in range(PIECES):
+                        send_result(layer, later, near)
+
+                @pl.when(jnp.logical_and(edge, jnp.logical_not(close)))
+                def _():
+                    send_aside(layer, p)
+
+        total = final_send if last else chip_total
+        load(3, layer).wait()
         for p in range(PIECES):
-            if merged(layer, p) and (layer > 0 or p == PIECES - 1):
-                merge(layer, p)
-        load(3, layer).wait()
-
+            merge(layer, p)
         for p in range(PIECES):
             out_project(layer, p)
-            if last:
-                final_send(layer, p)
-            else:
-                chip_total(layer, p)
+            total(layer, p)
         if not last:
             load(0, layer + 1).wait()
         for p in range(PIECES):
@@ -529,7 +543,7 @@
     return pl.pallas_call(
         functools.partial(fused_kernel, nx, sp, depth),
         out_shape=jax.ShapeDtypeStruct((trows, width), BF16),
-        in_specs=[anywhere] * 6 + [whole],
+        in_specs=[anywhere] * 7,
         out_specs=whole,
         scratch_shapes=[
             vmem((tp, trows, width), BF16),
@@ -539,7 +553,7 @@
             vmem(w_value.shape, BF16),
             vmem(w_out.shape, BF16),
             vmem((depth, units * rows, local_width), BF16),
-            vmem((depth, local_width, units * rows), BF16),
+            vmem((depth, units * rows, local_width), BF16),
             vmem((PIECES, tp, prows, width), F32),
             vmem((PIECES, tp, prows, width), BF16),
             vmem(results, BF16),
@@ -547,22 +561,24 @@
             vmem(results, BF16),
             vmem(notes, F32),
             vmem(notes, F32),
-            vmem(results[:2] + results[3:], BF16),
-            vmem(notes[:2] + notes[3:], F32),
+            vmem(results[:2] + (2,) + results[3:], BF16),
+            vmem(notes[:2] + (2,) + notes[3:], F32),
             vmem((piece_rows, local_width), BF16),
             vmem((depth, PIECES, CORES, nx, prows, width), BF16),
             vmem((depth, PIECES, nx, prows, width), BF16),
             vmem((depth, PIECES, nx, CORES, nx, prows, width), BF16),
             vmem((2, PIECES, nx, prows, width), BF16),
             vmem((1024, 8, 128), F32),
-            dma((2,)), dma((3, depth)), dma((3,)), dma((nx,)),
-            dma((units - 2, 2)), dma((1,)), dma((units - 2,)), dma((1,)), dma((depth - 1, PIECES, sp)),
-            dma((depth, PIECES)), dma((depth, PIECES)), dma((depth, PIECES)),
+            vmem(gains.shape, F32),
+            dma((3,)), dma((3, depth)), dma((3,)), dma((nx,)),
+            dma((units - 2, 4)), dma((1,)), dma((units - 2, 2)), dma((1,)), dma((depth - 1, PIECES, sp)),
+            dma((depth, PIECES)), dma((depth, PIECES, 2)), dma((depth, PIECES)),
             dma((depth - 1, PIECES, nx - 1)), dma((depth - 1, PIECES)), dma((PIECES, nx - 1)),
         ],
         compiler_params=pltpu.CompilerParams(
-            collective_id=0, has_side_effects=True, vmem_limit_bytes=60 * 1024 * 1024),
-    )(target, source, w_query, w_key, w_value, w_out, gains)
+            collective_id=0, has_side_effects=True, vmem_limit_bytes=VMEM_KIB * 1024),
+    )(*[pltpu.with_memory_space_constraint(one, pltpu.HBM) for one in (
+        target, source, w_query, w_key, w_value, w_out, gains)])
 
 
 def split_heads(row_block):
@@ -653,7 +669,7 @@
     def run(target, source, w_query, w_key, w_value, w_out, gains):
         trows, rows, local_width = target.shape[0], source.shape[0], w_query.shape[2]
         tiles = (trows % (16 * PIECES) == 0 and tp * trows == PIECES * (HEAD // 2) and rows % 128 == 0
-                 and sp % 2 == 0 and sp >= 4 and w_query.shape[0] > 1 and tp > CORES
+                 and sp % 2 == 0 and sp // 2 == 2 and w_query.shape[0] > 1 and tp > CORES
                  and local_width % (4 * HEAD) == 0 and tp % CORES == 0)
         form = functools.partial(fused_body, tp // CORES, sp) if tiles else body
         return form(target, source, w_query, w_key, w_value, w_out, gains)

time: 85.2 us -> 79.8 us (0.937)
  Pallas kernels: 83.4 us -> 78.9 us
  local copies, waits for them, and re-layouts: 1.57 us -> 0.66 us
    pallas_call x1, Pallas kernels: 83.4 us -> 78.9 us  [fused_body(): pl.pallas_call(functools.partial(fused_kernel, nx, sp, depth), out_shape=...]
    unnamed x1, local copies, waits for them, and re-layouts: 1.57 us -> 0.66 us
where the time goes in v3:
time: 79.8 us; the launch traced here: 79.6 us
  Pallas kernels  78.9 us (99%)
    pallas_call x1, Pallas kernels, fused_body(): pl.pallas_call(functools.partial(fused_kernel, nx, sp, depth), out_shape=...  78.9 us

profile of v3, /device:TPU:0, one launch (start us, length us, event | category | flops | bytes accessed | tf_op | source)
XLA Modules:
  0.0 79.6 jit_solution(5841634500877104895)
XLA Ops:
  0.0 78.9 %shard_map.73 = bf16[32,2048]{1,0:T(8,128)(2,1)S(1)} custom-call(bf16[32,2048]{1,0:T(8,128)(2,1)} %target.1, bf16[256,2048]{1,0:T(8,128)(2,1)} %source.1, bf16[2,2048,512]{2,1,0:T(8,128)(2,1)} %w_query.1, bf16[2,2048,512]{2,1,0:T(8,128)(2,1)} %w_key.1, bf16[2,2048,512]{2,1,0:T(8,128)(2,1)} %w_value.1, bf16[2,512,2048]{2,1,0:T(8,128)(2,1)} %w_out.1, ...), custom_call_target="tpu_custom_call" | custom-call | tf_op jit(solution)/shard_map/pallas_call | solution.py:543
  79.0 0.7 copy.9

commit v4 on v3

--- a/solution.py
+++ b/solution.py
@@ -11,7 +11,8 @@
 HEAD = 128
 CORES = 2
 PIECES = 2
-VMEM_KIB = 54100
+SWAPPED = 2
+VMEM_KIB = 50000
 
 
 EPS = 1e-06
@@ -34,7 +35,7 @@
     tbuf, sbuf, wq, wk, wv, wo, keys, values, stream, normed, qbuf,
     osend, orecv, ssend, srecv, orelay, srelay, attended, pbuf, half_in, chip_sum, fin, ledger, gains,
     local_sem, weight_sem, send_sem, t_recv, s_recv, p_recv, r_recv, first_recv, q_recv,
-    o_recv, m_recv, h_recv, c_recv, d_recv, f_recv,
+    x_recv, o_recv, m_recv, h_recv, c_recv, d_recv, f_recv,
 ):
     s = lax.axis_index("sp")
     t = lax.axis_index("tp")
@@ -110,13 +111,16 @@
     pl.semaphore_signal(barrier, inc=1, device_id=partner, device_id_type=MESH)
     for step in range(1, nx):
         pl.semaphore_signal(barrier, inc=1, device_id=peer(step), device_id_type=MESH)
+        pl.semaphore_signal(
+            barrier, inc=1, device_id={"tp": chip(step) * CORES + partner_c}, device_id_type=MESH)
     for step in range(1, sp):
         pl.semaphore_signal(
             barrier, inc=1, device_id={"sp": lax.rem(s + step, sp)}, device_id_type=MESH)
     with jax.named_scope("barrier"):
-        pl.semaphore_wait(barrier, 1 + (nx - 1) + (sp - 1))
+        pl.semaphore_wait(barrier, 1 + 2 * (nx - 1) + (sp - 1))
 
     spans = ((0, half // 2), (half // 2, half // 4), (3 * half // 4, half // 8), (7 * half // 8, half // 8))
+    swapped_rows = half - spans[SWAPPED][0]
     SOURCE, LINE, ROW = range(3)
     sent = {SOURCE: [], LINE: [], ROW: []}
 
@@ -134,9 +138,19 @@
             span = pl.ds(at, size)
             for step in range(1, nx):
                 unit = 2 * (nx - step) + part
-                go(remote(block.at[span], sbuf.at[unit, 0, span], send_sem.at[SOURCE],
-                          s_recv.at[unit - 2, piece], peer(step)),
-                   SOURCE, ((size, width), 2))
+                copy = remote(block.at[span], sbuf.at[unit, 0, span], send_sem.at[SOURCE],
+                              s_recv.at[unit - 2, piece], peer(step))
+                if part == 1 and piece >= SWAPPED:
+                    pl.when(c == 1)(copy.start)
+                    sent[SOURCE].append(((size, width), 2))
+
+                    @pl.when(c == 0)
+                    def _():
+                        remote(block.at[span], sbuf.at[unit, 1, span], send_sem.at[SOURCE],
+                               x_recv.at[nx - step - 1, piece - SWAPPED],
+                               {"tp": chip(step) * CORES + 1}).start()
+                else:
+                    go(copy, SOURCE, ((size, width), 2))
         go(remote(block, sbuf.at[1, part], send_sem.at[SOURCE], p_recv.at[0], partner),
            SOURCE, source_part)
 
@@ -172,6 +186,13 @@
                 arrived(q_recv.at[level - 1, p, block], result_block)
                 query_copy(level, p, block, near).start()
 
+    def hand_on(level, p):
+        forward(level, p)
+
+        @pl.when(jnp.logical_and(inner, p + 1 < PIECES))
+        def _():
+            query_copy(level, p + 1, s, near).start()
+
     def send_queries(level, p):
         if level == 0:
             query_copy(level, p, s, far_edge).start()
@@ -286,9 +307,33 @@
                 project_half(unit, level, 0)
 
             with jax.named_scope("wait_remote2"):
-                relay_pieces(unit, range(1, len(spans)))
+                relay_pieces(unit, range(1, SWAPPED))
+                shared = unit % 2 == 1
+
+                @pl.when(jnp.logical_or(c == 1, jnp.logical_not(shared)))
+                def _():
+                    relay_pieces(unit, range(SWAPPED, len(spans)))
+
+                @pl.when(jnp.logical_and(c == 1, shared))
+                def _():
+                    for piece in range(SWAPPED, len(spans)):
+                        span = pl.ds(*spans[piece])
+                        arrived(x_recv.at[(unit - 3) // 2, piece - SWAPPED], ((spans[piece][1], width), 2))
+                        remote(sbuf.at[unit, 1, span], sbuf.at[unit, 0, span], send_sem.at[SOURCE],
+                               r_recv.at[unit - 2, 1], partner).start()
+
             with jax.named_scope("wait_relayed"):
-                arrived(r_recv.at[unit - 2, 1], ((half // 2, width), 2))
+                @pl.when(jnp.logical_not(shared))
+                def _():
+                    arrived(r_recv.at[unit - 2, 1], ((half // 2, width), 2))
+
+                @pl.when(jnp.logical_and(c == 0, shared))
+                def _():
+                    arrived(r_recv.at[unit - 2, 1], ((half // 2 + swapped_rows, width), 2))
+
+                @pl.when(jnp.logical_and(c == 1, shared))
+                def _():
+                    arrived(r_recv.at[unit - 2, 1], ((half // 2 - swapped_rows, width), 2))
 
             @pl.when(unit == units - 1)
             def _():
@@ -298,7 +343,8 @@
         def _():
             project(index)
 
-    sent[SOURCE] += [source_part] * (units - 2)
+    sent[SOURCE] += [source_part] * (units - 2 - (nx - 1))
+    sent[SOURCE] += [((half - swapped_rows, width), 2)] * (nx - 1)
     arrived(first_recv.at[0], *([result_block] * (PIECES * (sp - 1))))
 
     def columns(parts):
@@ -445,6 +491,8 @@
     for layer in range(depth):
         last = layer == depth - 1
         own_pair = s // 2
+        if layer > 0:
+            hand_on(layer, 0)
         if layer == 1:
             @pl.loop(units * depth - (depth - 1), units * depth)
             def _(index):
@@ -471,11 +519,9 @@
 
                 @pl.when(close)
                 def _():
-                    forward(layer, p)
-
-                    @pl.when(jnp.logical_and(inner, p + 1 < PIECES))
+                    @pl.when(p > 0)
                     def _():
-                        query_copy(layer, p + 1, s, near).start()
+                        hand_on(layer, p)
 
                     with jax.named_scope("wait_near"):
                         arrived(q_recv.at[layer - 1, p, near], result_block)
@@ -522,8 +568,16 @@
 
     with jax.named_scope("finish"):
         drain_line()
-        for kind in (SOURCE, ROW):
-            arrived(send_sem.at[kind], *sent[kind])
+        arrived(send_sem.at[ROW], *sent[ROW])
+        moved = ((swapped_rows * (nx - 1), width), 2)
+
+        @pl.when(c == 0)
+        def _():
+            arrived(send_sem.at[SOURCE], *sent[SOURCE])
+
+        @pl.when(c == 1)
+        def _():
+            arrived(send_sem.at[SOURCE], *sent[SOURCE], moved, moved)
 
 
 def fused_body(nx, sp, target, source, w_query, w_key, w_value, w_out, gains):
@@ -572,6 +626,7 @@
             vmem(gains.shape, F32),
             dma((3,)), dma((3, depth)), dma((3,)), dma((nx,)),
             dma((units - 2, 4)), dma((1,)), dma((units - 2, 2)), dma((1,)), dma((depth - 1, PIECES, sp)),
+            dma((nx - 1, 4 - SWAPPED)),
             dma((depth, PIECES)), dma((depth, PIECES, 2)), dma((depth, PIECES)),
             dma((depth - 1, PIECES, nx - 1)), dma((depth - 1, PIECES)), dma((PIECES, nx - 1)),
         ],

time: 79.8 us -> 78.6 us (0.985)
  Pallas kernels: 78.9 us -> 77.8 us
    pallas_call x1, Pallas kernels: 78.9 us -> 77.8 us  [fused_body(): pl.pallas_call(functools.partial(fused_kernel, nx, sp, depth), out_shape=...]
where the time goes in v4:
time: 78.6 us; the launch traced here: 78.5 us
  Pallas kernels  77.8 us (99%)
    pallas_call x1, Pallas kernels, fused_body(): pl.pallas_call(functools.partial(fused_kernel, nx, sp, depth), out_shape=...  77.8 us

profile of v4, /device:TPU:0, one launch (start us, length us, event | category | flops | bytes accessed | tf_op | source)
XLA Modules:
  0.0 78.5 jit_solution(5527215068861929483)
XLA Ops:
  0.0 77.8 %shard_map.73 = bf16[32,2048]{1,0:T(8,128)(2,1)S(1)} custom-call(bf16[32,2048]{1,0:T(8,128)(2,1)} %target.1, bf16[256,2048]{1,0:T(8,128)(2,1)} %source.1, bf16[2,2048,512]{2,1,0:T(8,128)(2,1)} %w_query.1, bf16[2,2048,512]{2,1,0:T(8,128)(2,1)} %w_key.1, bf16[2,2048,512]{2,1,0:T(8,128)(2,1)} %w_value.1, bf16[2,512,2048]{2,1,0:T(8,128)(2,1)} %w_out.1, ...), custom_call_target="tpu_custom_call" | custom-call | tf_op jit(solution)/shard_map/pallas_call | solution.py:597
  77.8 0.7 copy.9

commit v5 on v4

--- a/solution.py
+++ b/solution.py
@@ -12,7 +12,7 @@
 CORES = 2
 PIECES = 2
 SWAPPED = 2
-VMEM_KIB = 50000
+VMEM_KIB = 54000
 
 
 EPS = 1e-06
@@ -34,6 +34,7 @@
     target, source, w_query, w_key, w_value, w_out, gain_rows, out,
     tbuf, sbuf, wq, wk, wv, wo, keys, values, stream, normed, qbuf,
     osend, orecv, ssend, srecv, orelay, srelay, attended, pbuf, half_in, chip_sum, fin, ledger, gains,
+    early_sum, early_peak, early_total,
     local_sem, weight_sem, send_sem, t_recv, s_recv, p_recv, r_recv, first_recv, q_recv,
     x_recv, o_recv, m_recv, h_recv, c_recv, d_recv, f_recv,
 ):
@@ -267,6 +268,34 @@
             qbuf[0, p, s] = q[p * piece_rows:(p + 1) * piece_rows].astype(BF16)
             send_queries(0, p)
 
+    own_pair = s // 2
+    every = slice(0, units * rows)
+    early = slice(0, (units - 1) * rows)
+    late = slice((units - 1) * rows, units * rows)
+
+    def head_scores(layer, q, h, span):
+        cols = slice(h * HEAD, (h + 1) * HEAD)
+        scores = lax.dot_general(
+            q[:, cols], keys[layer, span, cols], (((1,), (1,)), ((), ())), preferred_element_type=F32)
+        return scores, jnp.max(scores, axis=1, keepdims=True) * score_scale
+
+    def attend_early(p):
+        with jax.named_scope("attend_early"):
+            count = 2 * piece_rows
+            q = qbuf[0, p, pl.ds(2 * (1 - own_pair), 2)].reshape(count, local_width)
+            ahead = head_scores(0, q, 0, early)
+            for h in range(heads):
+                scores, peak = ahead
+                if h + 1 < heads:
+                    ahead = head_scores(0, q, h + 1, early)
+                cols = slice(h * HEAD, (h + 1) * HEAD)
+                weights = jnp.exp2(scores * score_scale - peak)
+                total = jnp.sum(weights, axis=1, keepdims=True)
+                early_sum[p, :, cols] = jnp.dot(
+                    weights.astype(BF16), values[0, early, cols], preferred_element_type=F32)
+                early_peak[p, :, cols] = jnp.broadcast_to(peak, (count, HEAD))
+                early_total[p, :, cols] = jnp.broadcast_to(total, (count, HEAD))
+
     @pl.loop(0, units * depth - (depth - 1))
     def _(index):
         unit = index // depth
@@ -296,6 +325,14 @@
                 first_queries()
             arrived(p_recv.at[0], source_part, source_part)
 
+        @pl.when(index == (units - 1) * depth)
+        def _():
+            arrived(first_recv.at[0], *([result_block] * (PIECES * (sp - 1))))
+
+            @pl.loop(0, PIECES)
+            def _(p):
+                attend_early(p)
+
         @pl.when(jnp.logical_and(unit >= 2, level == 0))
         def _():
             with jax.named_scope("wait_remote"):
@@ -345,7 +382,6 @@
 
     sent[SOURCE] += [source_part] * (units - 2 - (nx - 1))
     sent[SOURCE] += [((half - swapped_rows, width), 2)] * (nx - 1)
-    arrived(first_recv.at[0], *([result_block] * (PIECES * (sp - 1))))
 
     def columns(parts):
         stacked = jnp.concatenate(parts, axis=0)
@@ -377,27 +413,32 @@
                     ssend[layer, p, j] = jnp.concatenate([top, total], axis=0)
                     send_result(layer, p, j)
 
-    def head_scores(layer, q, h):
-        cols = slice(h * HEAD, (h + 1) * HEAD)
-        scores = lax.dot_general(
-            q[:, cols], keys[layer, :, cols], (((1,), (1,)), ((), ())), preferred_element_type=F32)
-        return scores, jnp.max(scores, axis=1, keepdims=True) * score_scale
-
-    def attend(layer, p, first, blocks):
+    def attend(layer, p, first, blocks, span, started=False):
         with jax.named_scope("attend"):
             count = blocks * piece_rows
             q = qbuf[layer, p, pl.ds(first, blocks)].reshape(count, local_width)
             lane = lax.broadcasted_iota(jnp.int32, (count, HEAD), 1)
             notes = jnp.zeros((count, HEAD), F32)
-            ahead = head_scores(layer, q, 0)
+            ahead = head_scores(layer, q, 0, span)
             for h in range(heads):
                 scores, peak = ahead
                 if h + 1 < heads:
-                    ahead = head_scores(layer, q, h + 1)
+                    ahead = head_scores(layer, q, h + 1, span)
                 cols = slice(h * HEAD, (h + 1) * HEAD)
-                weights = jnp.exp2(scores * score_scale - peak)
-                total = jnp.sum(weights, axis=1, keepdims=True)
-                o = jnp.dot(weights.astype(BF16), values[layer, :, cols], preferred_element_type=F32)
+                if started:
+                    before = early_peak[p, :, cols]
+                    peak = jnp.maximum(before, peak)
+                    fade = jnp.exp2(before - peak)
+                    shift = jnp.concatenate(
+                        [peak] * (scores.shape[1] // HEAD), axis=1)
+                    weights = jnp.exp2(scores * score_scale - shift)
+                    total = jnp.sum(weights, axis=1, keepdims=True) + fade * early_total[p, :, cols]
+                    o = jnp.dot(weights.astype(BF16), values[layer, span, cols], preferred_element_type=F32)
+                    o = o + fade * early_sum[p, :, cols]
+                else:
+                    weights = jnp.exp2(scores * score_scale - peak)
+                    total = jnp.sum(weights, axis=1, keepdims=True)
+                    o = jnp.dot(weights.astype(BF16), values[layer, span, cols], preferred_element_type=F32)
                 o = o.astype(BF16)
                 for member in range(blocks):
                     osend[layer, p, first + member, :, cols] = o[member * piece_rows:(member + 1) * piece_rows]
@@ -490,7 +531,6 @@
 
     for layer in range(depth):
         last = layer == depth - 1
-        own_pair = s // 2
         if layer > 0:
             hand_on(layer, 0)
         if layer == 1:
@@ -499,19 +539,19 @@
                 project(index)
 
         if layer == 0:
-            @pl.loop(0, 2 * PIECES)
-            def _(i):
-                p, far = i % PIECES, i < PIECES
-                attend(layer, p, jnp.where(far, 2 * (1 - own_pair), 2 * own_pair), 2)
-
-                @pl.when(jnp.logical_and(edge, far))
+            @pl.loop(0, PIECES)
+            def _(p):
+                attend(layer, p, 2 * (1 - own_pair), 2, late, started=True)
+
+                @pl.when(edge)
                 def _():
                     send_aside(layer, p)
 
-                @pl.when(jnp.logical_not(far))
-                def _():
-                    send_result(layer, p, near)
-                    keep_own(layer, p)
+            @pl.loop(0, PIECES)
+            def _(p):
+                attend(layer, p, 2 * own_pair, 2, every)
+                send_result(layer, p, near)
+                keep_own(layer, p)
         else:
             @pl.loop(0, 2 * PIECES)
             def _(i):
@@ -532,7 +572,7 @@
                         for block in (far_inner, far_edge):
                             arrived(q_recv.at[layer - 1, p, block], result_block)
 
-                attend(layer, p, jnp.where(close, 2 * own_pair, 2 * (1 - own_pair)), 2)
+                attend(layer, p, jnp.where(close, 2 * own_pair, 2 * (1 - own_pair)), 2, every)
 
                 @pl.when(close)
                 def _():
@@ -624,6 +664,9 @@
             vmem((2, PIECES, nx, prows, width), BF16),
             vmem((1024, 8, 128), F32),
             vmem(gains.shape, F32),
+            vmem((PIECES, 2 * piece_rows, local_width), F32),
+            vmem((PIECES, 2 * piece_rows, local_width), F32),
+            vmem((PIECES, 2 * piece_rows, local_width), F32),
             dma((3,)), dma((3, depth)), dma((3,)), dma((nx,)),
             dma((units - 2, 4)), dma((1,)), dma((units - 2, 2)), dma((1,)), dma((depth - 1, PIECES, sp)),
             dma((nx - 1, 4 - SWAPPED)),

time: 78.6 us -> 77.9 us (level)
  no operation moved by 1% of the time
where the time goes in v5:
time: 77.9 us; the launch traced here: 77.8 us
  Pallas kernels  77.1 us (99%)
    pallas_call x1, Pallas kernels, fused_body(): pl.pallas_call(functools.partial(fused_kernel, nx, sp, depth), out_shape=...  77.1 us

profile of v5, /device:TPU:0, one launch (start us, length us, event | category | flops | bytes accessed | tf_op | source)
XLA Modules:
  0.0 77.8 jit_solution(4720637990875569629)
XLA Ops:
  0.0 77.1 %shard_map.73 = bf16[32,2048]{1,0:T(8,128)(2,1)S(1)} custom-call(bf16[32,2048]{1,0:T(8,128)(2,1)} %target.1, bf16[256,2048]{1,0:T(8,128)(2,1)} %source.1, bf16[2,2048,512]{2,1,0:T(8,128)(2,1)} %w_query.1, bf16[2,2048,512]{2,1,0:T(8,128)(2,1)} %w_key.1, bf16[2,2048,512]{2,1,0:T(8,128)(2,1)} %w_value.1, bf16[2,512,2048]{2,1,0:T(8,128)(2,1)} %w_out.1, ...), custom_call_target="tpu_custom_call" | custom-call | tf_op jit(solution)/shard_map/pallas_call | solution.py:637
  77.1 0.7 copy.9

commit v6 on v5

--- a/solution.py
+++ b/solution.py
@@ -190,9 +190,10 @@
     def hand_on(level, p):
         forward(level, p)
 
-        @pl.when(jnp.logical_and(inner, p + 1 < PIECES))
-        def _():
-            query_copy(level, p + 1, s, near).start()
+        @pl.when(jnp.logical_and(inner, p == PIECES - 1))
+        def _():
+            for held in range(1, PIECES):
+                query_copy(level, held, s, near).start()
 
     def send_queries(level, p):
         if level == 0:
@@ -555,14 +556,15 @@
         else:
             @pl.loop(0, 2 * PIECES)
             def _(i):
-                p, close = i // 2, i % 2 == 0
+                p = i // 2
+                close = (i + jnp.where(jnp.logical_and(edge, p > 0), 1, 0)) % 2 == 0
+
+                @pl.when(jnp.logical_and(i % 2 == 1, p + 1 < PIECES))
+                def _():
+                    hand_on(layer, p + 1)
 
                 @pl.when(close)
                 def _():
-                    @pl.when(p > 0)
-                    def _():
-                        hand_on(layer, p)
-
                     with jax.named_scope("wait_near"):
                         arrived(q_recv.at[layer - 1, p, near], result_block)
 

time: 77.9 us -> 77.7 us (level)
  no operation moved by 1% of the time
where the time goes in v6:
time: 77.7 us; the launch traced here: 77.6 us
  Pallas kernels  76.9 us (99%)
    pallas_call x1, Pallas kernels, fused_body(): pl.pallas_call(functools.partial(fused_kernel, nx, sp, depth), out_shape=...  76.9 us

profile of v6, /device:TPU:0, one launch (start us, length us, event | category | flops | bytes accessed | tf_op | source)
XLA Modules:
  0.0 77.6 jit_solution(770109712735314052)
XLA Ops:
  0.0 76.9 %shard_map.73 = bf16[32,2048]{1,0:T(8,128)(2,1)S(1)} custom-call(bf16[32,2048]{1,0:T(8,128)(2,1)} %target.1, bf16[256,2048]{1,0:T(8,128)(2,1)} %source.1, bf16[2,2048,512]{2,1,0:T(8,128)(2,1)} %w_query.1, bf16[2,2048,512]{2,1,0:T(8,128)(2,1)} %w_key.1, bf16[2,2048,512]{2,1,0:T(8,128)(2,1)} %w_value.1, bf16[2,512,2048]{2,1,0:T(8,128)(2,1)} %w_out.1, ...), custom_call_target="tpu_custom_call" | custom-call | tf_op jit(solution)/shard_map/pallas_call | solution.py:639
  76.9 0.7 copy.9
